TPU v7x, 32 devices: a whole 2x2x4 slice. The times are simulated.
32 devices in a mesh: sp: 16 (over z, y, x), tp: 2 (over core).
Axes of the slice: x: 2, y: 2, z: 4, core: 2. Of those that a mesh axis runs over, the one named last changes fastest.
Arguments:
- tokens: bfloat16 [6144, 2048], P('sp', 'tp'), may hold values from -1620 to 1620
- input_norm_gain: float32 [2048], replicated, may hold values from 0.1 to 1.9
- outer_gate_weight: bfloat16 [2048, 1024], P(None, 'tp'), may hold values from -0.125 to 0.125
- inner_gate_weight: bfloat16 [2048, 1024], P(None, 'tp'), may hold values from -0.125 to 0.125
- convolution_input_weight: bfloat16 [2048, 1024], P(None, 'tp'), may hold values from -0.125 to 0.125
- convolution_kernel_taps: bfloat16 [3, 1024], P(None, 'tp'), may hold values from -3 to 3
- query_weight_matrix: bfloat16 [2048, 512], P(None, 'tp'), may hold values from -0.125 to 0.125
- key_weight_matrix: bfloat16 [2048, 512], P(None, 'tp'), may hold values from -0.125 to 0.125
- value_weight_matrix: bfloat16 [2048, 1024], P(None, 'tp'), may hold values from -0.125 to 0.125
- forget_gate_weight: bfloat16 [2048, 512], P(None, 'tp'), may hold values from -0.125 to 0.125
- attention_gate_weight: bfloat16 [2048, 1024], P(None, 'tp'), may hold values from -0.125 to 0.125
- forget_gate_bias: float32 [512], P('tp'), may hold values from -1.5 to 10
- extra_logarithm_decay: float32 [6144, 16], P('sp', 'tp'), may hold values from -0.72 to 0
- initial_head_state: float32 [16, 32, 64], P('tp'), may hold values from -768 to 768
- head_norm_gain: float32 [64], replicated, may hold values from 0.1 to 1.9
- convolution_output_weight: bfloat16 [1024, 2048], P('tp'), may hold values from -0.125 to 0.125
- attention_output_weight: bfloat16 [1024, 2048], P('tp'), may hold values from -0.125 to 0.125
Outputs:
- mixed: bfloat16 [6144, 2048], P(('sp', 'tp'))
All inputs are finite; a program needn't handle non-finite values.
Results may differ from a plain program's by a relative error of at most 0.017.
Values may be sent and summed in bfloat16 or wider, within the bound.
No kernel may reach another device: no remote copies, remote signals or barrier semaphores. Data moves between devices by JAX's collectives and lax.ppermute only.
A program may use at most 128 MiB of HBM per device.

v0:
```python
import functools

import jax
import jax.numpy as jnp
from jax import lax
from jax.experimental import pallas as pl
from jax.experimental.pallas import tpu as pltpu
from jax.sharding import PartitionSpec as P


BLOCK = 64
NORM_EPS = 1e-06
GATE_SOFTNESS = 16.0
F32 = jnp.float32
BF16 = jnp.bfloat16
NT = (((1,), (1,)), ((), ()))
TN = (((0,), (0,)), ((), ()))
VMEM = pl.BlockSpec(memory_space=pltpu.VMEM)
HBM = pl.BlockSpec(memory_space=pltpu.HBM)
EXTRA_ROWS = 8
CHUNKS = 4
FIRST = (2, 3, 1)
LAST = (3, 2, 1)


def dot(a, b):
    return jnp.dot(a, b, preferred_element_type=F32)


def call(body, outs, ins, flops, scratch=(), limit=12 << 20):
    specs = [s for _, s in ins]
    return pl.pallas_call(
        body,
        out_shape=[jax.ShapeDtypeStruct(s, d) for s, d in outs],
        in_specs=specs,
        out_specs=[VMEM] * len(outs),
        scratch_shapes=list(scratch),
        compiler_params=pltpu.CompilerParams(vmem_limit_bytes=limit),
        cost_estimate=pl.CostEstimate(flops=flops, bytes_accessed=1 << 20, transcendentals=0),
    )(*[pltpu.with_memory_space_constraint(a, pltpu.HBM) if s is HBM else a for a, s in ins])


def weight_copies(hbm, buf, sems, row, rows):
    copies, at = [], 0
    for i, w in enumerate(hbm):
        cols = w.shape[1]
        copies.append(
            pltpu.make_async_copy(
                w.at[pl.ds(row, rows), :], buf.at[:, at : at + cols], sems.at[i]
            )
        )
        at += cols
    return copies


def tile_lanes(column, lanes):
    return jnp.concatenate([column] * (lanes // column.shape[1]), axis=1)


def block_mask(rows, row_step, lanes, lane_step):
    r = lax.broadcasted_iota(jnp.int32, (rows, lanes), 0) // row_step
    c = lax.broadcasted_iota(jnp.int32, (rows, lanes), 1) // lane_step
    return r == c


def own_half(tok_hbm, gain_hbm, extra_hbm, *refs):
    n = len(refs) - 11
    weights, (acc, xg, ssq, wide, ahead) = refs[:n], refs[n : n + 5]
    buf, sems, tok, gain, extra, small = refs[n + 5 :]
    tp = lax.axis_index("tp")
    half = tok.shape[1]
    here = pl.multiple_of(tp * half, half)
    away = pl.multiple_of((1 - tp) * half, half)
    loads = [
        pltpu.make_async_copy(src, dst, small.at[i])
        for i, (src, dst) in enumerate([(extra_hbm, extra), (gain_hbm, gain), (tok_hbm, tok)])
    ]
    copies = weight_copies(weights, buf, sems.at[0], here, half)
    more = weight_copies(weights, ahead, sems.at[1], away, half)
    for c in loads + copies:
        c.start()
    loads[0].wait()
    loads[1].wait()
    loads[2].wait()
    for c in more:
        c.start()
    for c in copies:
        c.wait()
    heads = extra.shape[0]
    lanes = wide.shape[1]
    r = lax.broadcasted_iota(jnp.int32, (heads, lanes), 0)
    c = lax.broadcasted_iota(jnp.int32, (heads, lanes), 1) // (lanes // heads)
    wide[...] = lax.dot_general(
        extra[...],
        (r == c).astype(F32),
        TN,
        precision=lax.Precision.HIGHEST,
        preferred_element_type=F32,
    )
    x = tok[...].astype(F32)
    ssq[...] = jnp.broadcast_to(jnp.sum(x * x, axis=1, keepdims=True), ssq.shape)
    left = (x * gain[:, pl.ds(here, half)]).astype(BF16)
    xg[...] = left
    acc[...] = dot(left, buf[...])
    for c in more:
        c.wait()


def other_half(
    tok, gain, bias, acc, xg, ssq, wide, wnext, full, scale, key, val, cum, base, send
):
    tp = lax.axis_index("tp")
    rows, half = tok.shape
    here = pl.multiple_of(tp * half, half)
    away = pl.multiple_of((1 - tp) * half, half)
    x = tok[...].astype(F32)
    power = (ssq[:, :1] + jnp.sum(x * x, axis=1, keepdims=True)) * (0.5 / half)
    r = jnp.broadcast_to(lax.rsqrt(power + NORM_EPS), scale.shape)
    scale[...] = r
    left = (x * gain[:, pl.ds(away, half)]).astype(BF16)
    full[:, pl.ds(away, half)] = left
    full[:, pl.ds(here, half)] = xg[...]

    def project(lo, hi):
        s = acc[:, lo:hi] + dot(left, wnext[:, lo:hi])
        return (s * tile_lanes(r, hi - lo)).astype(BF16)

    kw, vw = key.shape[1], val.shape[1]
    k = project(0, kw)
    key[...] = k
    f = project(kw, 2 * kw).astype(F32) + bias[...]
    log = (jnp.minimum(f, 0.0) - jnp.log1p(jnp.exp(-jnp.abs(f)))) * (1.0 / GATE_SOFTNESS)
    log = log + wide[...]
    hi = log.astype(BF16)
    rest = log - hi.astype(F32)
    mid = rest.astype(BF16)
    low = (rest - mid.astype(F32)).astype(BF16)
    tri = (
        lax.broadcasted_iota(jnp.int32, (BLOCK, 3 * BLOCK), 0)
        >= lax.broadcasted_iota(jnp.int32, (BLOCK, 3 * BLOCK), 1) % BLOCK
    ).astype(BF16)
    n = rows // BLOCK
    running = jnp.zeros((1, kw), F32)
    starts, parts = [], []
    for b in range(n):
        s = slice(b * BLOCK, (b + 1) * BLOCK)
        part = dot(tri, jnp.concatenate([hi[s], mid[s], low[s]], axis=0))
        cum[s, :] = part
        parts.append(part)
        starts.append(running)
        running = running + part[BLOCK - 1 :]
    base[...] = jnp.concatenate(starts + [running] * (base.shape[0] - n), axis=0)
    kf = k.astype(F32)
    decayed = []
    for b in range(n):
        s = slice(b * BLOCK, (b + 1) * BLOCK)
        decayed.append((kf[s] * jnp.exp((running - starts[b]) - parts[b])).astype(BF16))
    decayed = jnp.concatenate(decayed, axis=0)
    v = project(2 * kw, 2 * kw + vw)
    val[...] = v
    dv = send.shape[0] - EXTRA_ROWS
    states = []
    for g in range(vw // 256):
        m = lax.dot_general(
            v[:, g * 256 : (g + 1) * 256],
            decayed[:, g * 128 : (g + 1) * 128],
            TN,
            preferred_element_type=F32,
        )
        states.append(fold(m, dv))
    pack(send, jnp.concatenate(states, axis=1), jnp.exp(running))


def fold(m, dv):
    step = m.shape[1] // (m.shape[0] // dv)
    lane = lax.broadcasted_iota(jnp.int32, (dv, m.shape[1]), 1) // step
    out = m[:dv]
    for h in range(1, m.shape[0] // dv):
        out = jnp.where(lane == h, m[h * dv : (h + 1) * dv], out)
    return out


def pack(ref, state, decay, halo=None):
    dv = state.shape[0]
    ref[:dv, :] = state.astype(BF16)
    top = decay.astype(BF16).astype(F32)
    row = lax.broadcasted_iota(jnp.int32, (EXTRA_ROWS, state.shape[1]), 0)
    tail = jnp.where(row == 0, top, decay - top)
    if halo is not None:
        tail = jnp.where(row < 2, tail, halo)
    ref[dv:, :] = tail.astype(BF16)


def unpack(v, dv):
    tail = v[dv:].astype(F32)
    return v[:dv].astype(F32), tail[0:1] + tail[1:2], tail


def to_tail(last):
    width = last.shape[1] // 2
    row = lax.broadcasted_iota(jnp.int32, (EXTRA_ROWS, width), 0)
    tail = jnp.zeros((EXTRA_ROWS, width), F32)
    end = last.shape[0]
    for i in range(4):
        at = end - 2 + i // 2
        part = last[at : at + 1, (i % 2) * width : (i % 2 + 1) * width]
        tail = jnp.where(row == 2 + i, part, tail)
    return tail


def from_tail(tail):
    return jnp.concatenate(
        [
            jnp.concatenate([tail[2:3], tail[3:4]], axis=1),
            jnp.concatenate([tail[4:5], tail[5:6]], axis=1),
        ],
        axis=0,
    )


def fill(stack, items):
    for i, item in enumerate(items):
        stack[i] = item[...]


def halo_of_round(halo, stack, radix, stride, digit, dv):
    low_zero = lax.rem(lax.axis_index("sp"), stride) == 0
    for j in range(radix - 1):
        tail = stack[j ^ digit][dv:].astype(F32)
        halo = jnp.where((j + 1 == digit) & low_zero, tail, halo)
    return halo


def before_round(pre, dv, lanes):
    if pre is None:
        return (
            jnp.zeros((dv, lanes), F32),
            jnp.ones((1, lanes), F32),
            jnp.zeros((EXTRA_ROWS, lanes), F32),
        )
    return unpack(pre[...], dv)


def join_round(radix, stride, *refs):
    items, pre, (send, pre_out, stack) = refs[:radix], refs[radix:-3], refs[-3:]
    dv = send.shape[0] - EXTRA_ROWS
    fill(stack, items)
    digit = lax.rem(lax.axis_index("sp") // stride, radix)
    lanes = stack.shape[2]
    had_s, had_d, had_halo = before_round(pre[0] if pre else None, dv, lanes)
    pre_s, pre_d = jnp.zeros((dv, lanes), F32), jnp.ones((1, lanes), F32)
    tot_s, tot_d = pre_s, pre_d
    for j in range(radix):
        s, d, tail = unpack(stack[j ^ digit], dv)
        before = j < digit
        pre_s = jnp.where(before, d * pre_s + s, pre_s)
        pre_d = jnp.where(before, d * pre_d, pre_d)
        tot_s, tot_d = d * tot_s + s, d * tot_d
    halo = halo_of_round(had_halo, stack, radix, stride, digit, dv)
    pack(pre_out, had_d * pre_s + had_s, had_d * pre_d, halo)
    pack(send, tot_s, tot_d, tail)


def scaled(x, w, r):
    s = dot(x, w)
    return (s * tile_lanes(r, s.shape[1])).astype(BF16)


def conv_inputs(full, scale, wc, wh, send, prod, out):
    r = scale[...]
    x = full[...]
    p = scaled(x, wc[...], r).astype(F32) * scaled(x, wh[...], r).astype(F32)
    p = p.astype(BF16)
    prod[...] = p
    dv = send.shape[0] - EXTRA_ROWS
    tail = to_tail(p[p.shape[0] - 16 :].astype(F32))
    row = lax.broadcasted_iota(jnp.int32, tail.shape, 0)
    out[:dv, :] = send[:dv, :]
    out[dv:, :] = jnp.where(row < 2, send[dv:, :].astype(F32), tail).astype(BF16)


def late_half(full, scale, taps, wb, wq, prod, query, outer, conv):
    r = scale[...]
    x = full[...]
    b = scaled(x, wb[...], r)
    outer[...] = b
    p = prod[...].astype(F32)
    row = lax.broadcasted_iota(jnp.int32, p.shape, 0)
    t = taps[...].astype(F32)
    total = jnp.zeros(p.shape, F32)
    for j in range(taps.shape[0] - 1):
        back = taps.shape[0] - 1 - j
        total = total + t[j : j + 1] * jnp.where(row >= back, pltpu.roll(p, back, 0), 0.0)
    total = total + t[taps.shape[0] - 1 :] * p
    conv[...] = (b.astype(F32) * total).astype(BF16)
    query[...] = scaled(x, wq[...], r)


def blockwise(
    key_dim, query, key, val, cum, base, start, full, scale, wg, gain, raw, through, first, gate
):
    rows = query.shape[0]
    n = rows // BLOCK
    shrink = key_dim**-0.5
    first[...] = start[...].T
    gated = scaled(full[...], wg[...], scale[...]).astype(F32)
    gate[...] = gated * jax.nn.sigmoid(gated) * tile_lanes(gain[...], gated.shape[1])
    k_mask = block_mask(256, 64, 128, 32)
    v_mask = block_mask(256, 64, 256, 64)
    causal = lax.broadcasted_iota(jnp.int32, (BLOCK, 256), 0) >= (
        lax.broadcasted_iota(jnp.int32, (BLOCK, 256), 1) % BLOCK
    )
    zero = jnp.zeros((), BF16)
    for g in range(val.shape[1] // 256):
        kl = slice(g * 128, (g + 1) * 128)
        vl = slice(g * 256, (g + 1) * 256)
        state = None
        for b in range(n):
            s = slice(b * BLOCK, (b + 1) * BLOCK)
            c = cum[s, kl]
            q = query[s, kl].astype(F32) * shrink
            k = key[s, kl].astype(F32)
            end = c[BLOCK - 1 :]
            q_in = (q * jnp.exp(c)).astype(BF16)
            k_in = (k * jnp.exp(-c)).astype(BF16)
            through[s, kl] = (q * jnp.exp(c + base[b : b + 1, kl])).astype(BF16)
            v = val[s, vl]
            k_wide = jnp.where(k_mask, jnp.concatenate([k_in] * 4, axis=0), zero)
            scores = lax.dot_general(q_in, k_wide, NT, preferred_element_type=F32)
            scores = jnp.where(causal, scores, 0.0).astype(BF16)
            v_wide = jnp.where(v_mask, jnp.concatenate([v] * 4, axis=0), zero)
            out = dot(scores, v_wide)
            if state is not None:
                out = out + lax.dot_general(
                    q_in, state.astype(BF16), NT, preferred_element_type=F32
                )
            raw[s, vl] = out
            if b < n - 1:
                k_out = (k * jnp.exp(end - c)).astype(BF16)
                new = lax.dot_general(v, k_out, TN, preferred_element_type=F32)
                new = jnp.where(k_mask, new, 0.0)
                state = new if state is None else state * jnp.exp(end) + new


def rows_out(half, incoming, halo, raw, through, gate, conv, outer, prod, taps):
    rows = raw.shape[0] // 2
    at = pl.multiple_of(half * rows, 64)
    here = pl.ds(at, rows)
    ones = block_mask(256, 64, 256, 64).astype(BF16) * (1.0 / 64)
    ones = ones.astype(BF16)
    parts = []
    for g in range(raw.shape[1] // 256):
        vl = slice(g * 256, (g + 1) * 256)
        x = raw[here, vl] + lax.dot_general(
            through[here, g * 128 : (g + 1) * 128],
            incoming[g],
            NT,
            preferred_element_type=F32,
        )
        mean = dot((x * x).astype(BF16), ones)
        parts.append((x * lax.rsqrt(mean + NORM_EPS) * gate[here, vl]).astype(BF16))
    attn = jnp.concatenate(parts, axis=1)
    p = prod[:16, :].astype(F32)
    row = lax.broadcasted_iota(jnp.int32, p.shape, 0)
    t = taps[...].astype(F32)
    back2 = jnp.where(row == 0, halo[0:1], jnp.where(row == 1, halo[1:2], pltpu.roll(p, 2, 0)))
    back1 = jnp.where(row == 0, halo[1:2], pltpu.roll(p, 1, 0))
    top = outer[:16, :].astype(F32) * (t[0:1] * back2 + t[1:2] * back1 + t[2:3] * p)
    mine = conv[here, :]
    head = jnp.where(half == 0, top, mine[:16].astype(F32)).astype(BF16)
    left = jnp.concatenate([head, mine[16:]], axis=0)
    return left, attn


def project_out(left, attn, wc, wa, out, skip=0):
    step = 512
    for n in range(0, out.shape[1], step):
        at = slice(skip + n, skip + n + step)
        s = dot(left, wc[:, at]) + dot(attn, wa[:, at])
        out[:, n : n + step] = s.astype(out.dtype)


def partner_rows(radix, stride, *refs):
    items, pre = refs[:radix], refs[radix:-16]
    first, raw, through, gate, conv, outer, prod, taps, wc, wa = refs[-16:-6]
    out, left_out, attn_out, state, halo_out, stack = refs[-6:]
    dv = first.shape[0]
    fill(stack, items)
    digit = lax.rem(lax.axis_index("sp") // stride, radix)
    lanes = stack.shape[2]
    had_s, had_d, had_halo = before_round(pre[0] if pre else None, dv, lanes)
    pre_s = first[...]
    for j in range(radix - 1):
        s, d, _ = unpack(stack[j ^ digit], dv)
        pre_s = jnp.where(j < digit, d * pre_s + s, pre_s)
    pre_s = had_d * pre_s + had_s
    mask = block_mask(256, 64, 128, 32)
    incoming = []
    for g in range(lanes // 128):
        s = pre_s[:, g * 128 : (g + 1) * 128]
        wide = jnp.where(mask, jnp.concatenate([s] * 4, axis=0), 0.0).astype(BF16)
        incoming.append(wide)
        state[g] = wide
    halo = from_tail(halo_of_round(had_halo, stack, radix, stride, digit, dv))
    halo_out[...] = jnp.concatenate([halo] * 4, axis=0)
    half = 1 - lax.axis_index("tp")
    left, attn = rows_out(half, incoming, halo, raw, through, gate, conv, outer, prod, taps)
    left_out[...] = left
    attn_out[...] = attn
    project_out(left, attn, wc, wa, out)


def partner_rest(left, attn, wc, wa, out):
    project_out(left[...], attn[...], wc, wa, out, out.shape[1])


def add_rows(mine, first, second, out_hbm, buf, sems):
    chunks = buf.shape[0]
    rows = buf.shape[1]
    width = first.shape[1]
    copies = []
    for i in range(chunks):
        here = slice(i * rows, (i + 1) * rows)
        buf[i, :, :width] = (mine[here, :width] + first[here, :].astype(F32)).astype(BF16)
        buf[i, :, width:] = (mine[here, width:] + second[here, :].astype(F32)).astype(BF16)
        copies.append(pltpu.make_async_copy(buf.at[i], out_hbm.at[here, :], sems.at[i]))
        copies[-1].start()
    for c in copies:
        c.wait()


def own_rows(state, halo, raw, through, gate, conv, outer, prod, taps, wc, wa, out):
    incoming = [state[g] for g in range(state.shape[0])]
    half = lax.axis_index("tp")
    left, attn = rows_out(
        half, incoming, halo[0:2, :], raw, through, gate, conv, outer, prod, taps
    )
    project_out(left, attn, wc, wa, out)


def radices(n):
    found = []
    while n > 1:
        r = 4 if n % 4 == 0 else 2
        found.append(r)
        n //= r
    return found


def on_device(
    tokens,
    input_norm_gain,
    outer_gate_weight,
    inner_gate_weight,
    convolution_input_weight,
    convolution_kernel_taps,
    query_weight_matrix,
    key_weight_matrix,
    value_weight_matrix,
    forget_gate_weight,
    attention_gate_weight,
    forget_gate_bias,
    extra_logarithm_decay,
    initial_head_state,
    head_norm_gain,
    convolution_output_weight,
    attention_output_weight,
):
    rows, half = tokens.shape
    heads, dk, dv = initial_head_state.shape
    kw, vw, cw = heads * dk, heads * dv, outer_gate_weight.shape[1]
    model = convolution_output_weight.shape[1]
    n_sp = lax.axis_size("sp")
    swap = [(0, 1), (1, 0)]
    other = lax.ppermute(tokens, "tp", swap)
    gain = input_norm_gain.reshape(1, -1)
    early = (key_weight_matrix, forget_gate_weight, value_weight_matrix)
    width = sum(w.shape[1] for w in early)
    extra = extra_logarithm_decay.T
    flops = 2 * rows * half * width
    acc, xg, ssq, wide, ahead = call(
        own_half,
        [
            ((rows, width), F32),
            ((rows, half), BF16),
            ((rows, 128), F32),
            ((rows, kw), F32),
            ((half, width), BF16),
        ],
        [(tokens, HBM), (gain, HBM), (extra, HBM)] + [(w, HBM) for w in early],
        flops,
        [
            pltpu.VMEM((half, width), BF16),
            pltpu.SemaphoreType.DMA((2, len(early))),
            pltpu.VMEM(tokens.shape, BF16),
            pltpu.VMEM(gain.shape, F32),
            pltpu.VMEM(extra.shape, F32),
            pltpu.SemaphoreType.DMA((3,)),
        ],
    )
    full, scale, key, val, cum, base, send = call(
        other_half,
        [
            ((rows, 2 * half), BF16),
            ((rows, 128), F32),
            ((rows, kw), BF16),
            ((rows, vw), BF16),
            ((rows, kw), F32),
            ((8, kw), F32),
            ((dv + EXTRA_ROWS, kw), BF16),
        ],
        [(other, VMEM), (gain, VMEM), (forget_gate_bias.reshape(1, -1), VMEM)]
        + [(a, VMEM) for a in (acc, xg, ssq, wide, ahead)],
        flops,
    )
    prod, send_halo = call(
        conv_inputs,
        [((rows, cw), BF16), (send.shape, BF16)],
        [(a, VMEM) for a in (full, scale, inner_gate_weight, convolution_input_weight, send)],
        2 * rows * 2 * half * 2 * cw,
    )
    query, outer, conv = call(
        late_half,
        [((rows, kw), BF16), ((rows, cw), BF16), ((rows, cw), BF16)],
        [
            (a, VMEM)
            for a in (
                full,
                scale,
                convolution_kernel_taps,
                outer_gate_weight,
                query_weight_matrix,
                prod,
            )
        ],
        2 * rows * 2 * half * (kw + cw),
    )
    raw, through, first, gate = call(
        functools.partial(blockwise, dk),
        [((rows, vw), F32), ((rows, kw), BF16), ((dv, kw), F32), ((rows, vw), F32)],
        [
            (a, VMEM)
            for a in (
                query,
                key,
                val,
                cum,
                base,
                initial_head_state.reshape(heads * dk, dv),
                full,
                scale,
                attention_gate_weight,
                head_norm_gain.reshape(1, -1),
            )
        ],
        2 * rows * 2 * half * (kw + vw),
    )
    pre = ()
    stride = 1
    plan = radices(n_sp)
    crossed = len(plan) % 2 == 0
    for turn, radix in enumerate(plan):
        items = [send] + [None] * (radix - 1)
        for j in FIRST if turn == 0 else LAST if radix == 4 else range(1, radix):
            pairs = [
                (2 * i + c, 2 * (i ^ (j * stride)) + (1 - c if crossed else c))
                for i in range(n_sp)
                for c in range(2)
            ]
            payload = send_halo if turn == 0 and j % 2 == 1 else send
            items[j] = lax.ppermute(payload, ("sp", "tp"), pairs)
        if crossed and turn < len(plan) - 1:
            items[0] = lax.ppermute(send, "tp", swap)
        if crossed and turn > 0:
            pre = (lax.ppermute(pre[0], "tp", swap),)
        stack = [pltpu.VMEM((radix,) + send.shape, BF16)]
        if turn < len(plan) - 1:
            send, *pre = call(
                functools.partial(join_round, radix, stride),
                [(send.shape, BF16), (send.shape, BF16)],
                [(a, VMEM) for a in (*items, *pre)],
                1 << 20,
                stack,
            )
            stride *= radix
    tail = [
        (a, VMEM)
        for a in (
            raw,
            through,
            gate,
            conv,
            outer,
            prod,
            convolution_kernel_taps,
            convolution_output_weight,
            attention_output_weight,
        )
    ]
    flops = 2 * (rows // 2) * model * (vw + cw)
    theirs, left, attn, state, halo = call(
        functools.partial(partner_rows, plan[-1], stride),
        [
            ((rows // 2, model // 2), BF16),
            ((rows // 2, cw), BF16),
            ((rows // 2, vw), BF16),
            ((kw // 128, 256, 128), BF16),
            ((8, cw), F32),
        ],
        [(a, VMEM) for a in (*items, *pre, first)] + tail,
        flops // 2,
        stack,
    )
    got_first = lax.ppermute(theirs, "tp", swap)
    (theirs,) = call(
        partner_rest,
        [((rows // 2, model // 2), BF16)],
        [
            (a, VMEM)
            for a in (left, attn, convolution_output_weight, attention_output_weight)
        ],
        flops // 2,
    )
    got_second = lax.ppermute(theirs, "tp", swap)
    (mine,) = call(
        own_rows, [((rows // 2, model), F32)], [(state, VMEM), (halo, VMEM)] + tail, flops
    )
    return pl.pallas_call(
        add_rows,
        out_shape=jax.ShapeDtypeStruct((rows // 2, model), BF16),
        in_specs=[VMEM] * 3,
        out_specs=HBM,
        scratch_shapes=[
            pltpu.VMEM((CHUNKS, rows // 2 // CHUNKS, model), BF16),
            pltpu.SemaphoreType.DMA((CHUNKS,)),
        ],
        compiler_params=pltpu.CompilerParams(vmem_limit_bytes=12 << 20),
        cost_estimate=pl.CostEstimate(flops=1 << 20, bytes_accessed=1 << 20, transcendentals=0),
        name="add_rows",
    )(mine, got_first, got_second)


def solution(mesh):
    placed = (
        P("sp", "tp"),
        P(),
        P(None, "tp"),
        P(None, "tp"),
        P(None, "tp"),
        P(None, "tp"),
        P(None, "tp"),
        P(None, "tp"),
        P(None, "tp"),
        P(None, "tp"),
        P(None, "tp"),
        P("tp"),
        P("sp", "tp"),
        P("tp", None, None),
        P(),
        P("tp", None),
        P("tp", None),
    )

    return jax.shard_map(
        on_device, mesh=mesh, in_specs=placed, out_specs=P(("sp", "tp"), None), check_vma=False
    )
```

profile of v0, /device:TPU:0, one launch (start us, length us, event | category | flops | bytes accessed | tf_op | source)
XLA Modules:
  0.0 28.2 jit_solution(2243780059020716653)
XLA Ops:
  0.0 0.5 %collective-permute-start = (bf16[384,1024]{1,0:T(8,128)(2,1)}, bf16[384,1024]{1,0:T(8,128)(2,1)S(1)}, u32[]{:S(2)}, u32[]{:S(2)}) collective-permute-start(bf16[384,1024]{1,0:T(8,128)(2,1)} %tok_hbm.1), channel_id=1, source_target_pairs={{0,1},{1,0},{2,3},{3,2},{4,5},{5,4},{6,7},{7,6},{8,9},{9,8},{10,11... | collective-permute-start | bytes 2359304 | tf_op jit(solution)/shard_map/ppermute | solution.py:475
  0.5 3.3 %shard_map.163 = (f32[384,1024]{1,0:T(8,128)S(1)}, bf16[384,1024]{1,0:T(8,128)(2,1)S(1)}, f32[384,128]{1,0:T(8,128)S(1)}, f32[384,256]{1,0:T(8,128)S(1)}, bf16[1024,1024]{1,0:T(8,128)(2,1)S(1)}) custom-call(bf16[384,1024]{1,0:T(8,128)(2,1)} %tok_hbm.1, f32[1,2048]{1,0:T(1,128)} %bitcast.6, f32[8,384]{1,0:T(8,128)} %bitcast.10, bf16[2048,256]{1,0:T(8,128)(2,1)} %refs_0_.1, ...), custom_call_target="tpu_custom_call" | custom-call | flops 805306368 | bytes 1048576 | tf_op jit(solution)/shard_map/pallas_call | solution.py:32
  3.8 0.0 collective-permute-done.tok
  3.8 0.0 copy-done.9
  3.8 0.0 copy-done.10
  3.8 0.0 copy-start.2
  3.8 0.0 copy-start.3
  3.8 1.9 %shard_map.164 = (bf16[384,2048]{1,0:T(8,128)(2,1)S(1)}, f32[384,128]{1,0:T(8,128)S(1)}, bf16[384,256]{1,0:T(8,128)(2,1)S(1)}, bf16[384,512]{1,0:T(8,128)(2,1)S(...) custom-call(bf16[384,1024]{1,0:T(8,128)(2,1)S(1)} %collective-permute-done.tok, ...), custom_call_target="tpu_custom_call" | custom-call | flops 805306368 | bytes 1048576 | tf_op jit(solution)/shard_map/pallas_call | solution.py:32
  5.7 2.7 %collective-permute-start.3 = (bf16[72,256]{1,0:T(8,128)(2,1)S(1)}, bf16[72,256]{1,0:T(8,128)(2,1)S(1)}, u32[]{:S(2)}, u32[]{:S(2)}) collective-permute-start(bf16[72,256]{1,0:T(8,128)(2,1)S(1)} %get-tuple-element.38.send), channel_id=1, source_target_pairs={{0,5},{1,4},{2,7},{3,6},{4,1},{5,0},{6,3},{7,2},{8,13},{9,12},{10,... | collective-permute-start | bytes 110600 | tf_op jit(solution)/shard_map/ppermute | solution.py:571
  8.4 0.0 collective-permute-start.1
  8.4 0.0 copy-done.2
  8.4 0.0 copy-done.3
  8.4 0.0 copy-start.6
  8.4 0.0 copy-start.8
  8.5 1.9 %shard_map.165 = (bf16[384,512]{1,0:T(8,128)(2,1)S(1)}, bf16[72,256]{1,0:T(8,128)(2,1)S(1)}) custom-call(bf16[384,2048]{1,0:T(8,128)(2,1)S(1)} %get-tuple-element.39.full, f32[384,128]{1,0:T(8,128)S(1)} %get-tuple-element.40.scale, bf16[2048,512]{1,0:T(8,128)(2,1)S(1)} %copy-done.2, bf16[2048,512]{1,0:T(8,128)(2,1)S(1)} %copy-done.3, ...), custom_call_target="tpu_custom_call" | custom-call | flops 1610612736 | bytes 1048576 | tf_op jit(solution)/shard_map/pallas_call | solution.py:32
  10.3 1.6 %collective-permute-start.4 = (bf16[72,256]{1,0:T(8,128)(2,1)S(1)}, bf16[72,256]{1,0:T(8,128)(2,1)S(1)}, u32[]{:S(2)}, u32[]{:S(2)}) collective-permute-start(bf16[72,256]{1,0:T(8,128)(2,1)S(1)} %get-tuple-element.41), channel_id=1, source_target_pairs={{0,7},{1,6},{2,5},{3,4},{4,3},{5,2},{6,1},{7,0},{8,15},{9,14},{10,... | collective-permute-start | bytes 110600 | tf_op jit(solution)/shard_map/ppermute | solution.py:571
  11.9 0.1 collective-permute-start.2
  12.1 0.0 copy-done.4
  12.1 0.0 copy-done.6
  12.1 0.0 copy-done.8
  12.1 0.0 copy-start.7
  12.1 0.0 copy-start.11
  12.1 1.5 %shard_map.167 = (bf16[384,256]{1,0:T(8,128)(2,1)S(1)}, bf16[384,512]{1,0:T(8,128)(2,1)S(1)}, bf16[384,512]{1,0:T(8,128)(2,1)S(1)}) custom-call(bf16[384,2048]{1,0:T(8,128)(2,1)S(1)} %get-tuple-element.39.full, f32[384,128]{1,0:T(8,128)S(1)} %get-tuple-element.40.scale, bf16[3,512]{1,0:T(4,128)(2,1)S(1)} %copy-done.8, bf16[2048,512]{1,0:T(8,128)(2,1)S(1)} %copy-done.4, ...), custom_call_target="tpu_custom_call" | custom-call | flops 1207959552 | bytes 1048576 | tf_op jit(solution)/shard_map/pallas_call | solution.py:32
  13.6 0.0 collective-permute-done.3.refs_2_
  13.6 0.0 collective-permute-done.1.refs_0_
  13.6 1.1 %collective-permute-done.4.refs_3_ = bf16[72,256]{1,0:T(8,128)(2,1)S(1)} collective-permute-done((bf16[72,256]{1,0:T(8,128)(2,1)S(1)}, bf16[72,256]{1,0:T(8,128)(2,1)S(1)}, u32[]{:S(2)}, u32[]{:S(2)}) %collective-permute-start.4) | collective-permute-done | bytes 36896 | tf_op jit(solution)/shard_map/ppermute | solution.py:571
  14.7 0.8 %collective-permute-done.2.refs_1_ = bf16[72,256]{1,0:T(8,128)(2,1)S(1)} collective-permute-done((bf16[72,256]{1,0:T(8,128)(2,1)S(1)}, bf16[72,256]{1,0:T(8,128)(2,1)S(1)}, u32[]{:S(2)}, u32[]{:S(2)}) %collective-permute-start.2) | collective-permute-done | bytes 36896 | tf_op jit(solution)/shard_map/ppermute | solution.py:571
  15.5 0.1 shard_map.166
  15.6 3.4 %collective-permute-start.7 = (bf16[72,256]{1,0:T(8,128)(2,1)S(1)}, bf16[72,256]{1,0:T(8,128)(2,1)S(1)}, u32[]{:S(2)}, u32[]{:S(2)}) collective-permute-start(bf16[72,256]{1,0:T(8,128)(2,1)S(1)} %get-tuple-element.42.refs_0_), channel_id=1, source_target_pairs={{0,25},{1,24},{2,27},{3,26},{4,29},{5,28},{6,31},{7,30},{8,17},{9,... | collective-permute-start | bytes 110600 | tf_op jit(solution)/shard_map/ppermute | solution.py:571
  19.0 0.0 collective-permute-start.6
  19.0 0.6 %collective-permute-start.5 = (bf16[72,256]{1,0:T(8,128)(2,1)S(1)}, bf16[72,256]{1,0:T(8,128)(2,1)S(1)}, u32[]{:S(2)}, u32[]{:S(2)}) collective-permute-start(bf16[72,256]{1,0:T(8,128)(2,1)S(1)} %get-tuple-element.42.refs_0_), channel_id=1, source_target_pairs={{0,9},{1,8},{2,11},{3,10},{4,13},{5,12},{6,15},{7,14},{8,1},{9,0},... | collective-permute-start | bytes 110600 | tf_op jit(solution)/shard_map/ppermute | solution.py:571
  19.6 0.2 collective-permute-start.8
  19.9 0.0 copy-done.5
  19.9 0.0 copy-done.11
  19.9 0.0 copy-start.1
  19.9 2.4 %shard_map.168 = (f32[384,512]{1,0:T(8,128)S(1)}, bf16[384,256]{1,0:T(8,128)(2,1)S(1)}, f32[64,256]{1,0:T(8,128)S(1)}, f32[384,512]{1,0:T(8,128)S(1)}) custom-call(bf16[384,256]{1,0:T(8,128)(2,1)S(1)} %get-tuple-element.45.query, bf16[384,256]{1,0:T(8,128)(2,1)S(1)} %get-tuple-element.46.key, bf16[384,512]{1,0:T(8,128)(2,1)S(1)} %get-tuple-element.47.val, ...), custom_call_target="tpu_custom_call" | custom-call | flops 1207959552 | bytes 1048576 | tf_op jit(solution)/shard_map/pallas_call | solution.py:32
  22.3 0.0 collective-permute-done.8.refs_4_
  22.3 0.0 collective-permute-done.7.refs_3_
  22.3 1.0 %collective-permute-done.6.refs_2_ = bf16[72,256]{1,0:T(8,128)(2,1)S(1)} collective-permute-done((bf16[72,256]{1,0:T(8,128)(2,1)S(1)}, bf16[72,256]{1,0:T(8,128)(2,1)S(1)}, u32[]{:S(2)}, u32[]{:S(2)}) %collective-permute-start.6) | collective-permute-done | bytes 36896 | tf_op jit(solution)/shard_map/ppermute | solution.py:571
  23.3 0.0 collective-permute-done.5.refs_1_
  23.3 0.9 %shard_map.169 = (bf16[192,1024]{1,0:T(8,128)(2,1)S(1)}, bf16[192,512]{1,0:T(8,128)(2,1)S(1)}, bf16[192,512]{1,0:T(8,128)(2,1)S(1)}, bf16[2,256,128]{2,1,0:T(8,128)(2,1)S(1)}, f32[8,512]{1,0:T(8,128)S(1)}) custom-call(bf16[72,256]{1,0:T(8,128)(2,1)S(1)} %get-tuple-element.42.refs_0_, bf16[72,256]{1,0:T(8,128)(2,1)S(1)} %collective-permute-done.5.refs_1_, ...), custom_call_target="tpu_custom_call" | custom-call | flops 402653184 | bytes 1048576 | tf_op jit(solution)/shard_map/pallas_call | solution.py:32
  24.3 0.6 %shard_map.171 = bf16[192,1024]{1,0:T(8,128)(2,1)S(1)} custom-call(bf16[192,512]{1,0:T(8,128)(2,1)S(1)} %get-tuple-element.59.left, bf16[192,512]{1,0:T(8,128)(2,1)S(1)} %get-tuple-element.60.attn, bf16[512,2048]{1,0:T(8,128)(2,1)S(1)} %copy-done, bf16[512,2048]{1,0:T(8,128)(2,1)S(1)} %copy-done.1), custom_call_target="tpu_custom_call" | custom-call | flops 402653184 | bytes 1048576 | tf_op jit(solution)/shard_map/pallas_call | solution.py:32
  24.9 0.4 %collective-permute-start.10 = (bf16[192,1024]{1,0:T(8,128)(2,1)S(1)}, bf16[192,1024]{1,0:T(8,128)(2,1)S(1)}, u32[]{:S(2)}, u32[]{:S(2)}) collective-permute-start(bf16[192,1024]{1,0:T(8,128)(2,1)S(1)} %shard_map.171), channel_id=1, source_target_pairs={{0,1},{1,0},{2,3},{3,2},{4,5},{5,4},{6,7},{7,6},{8,9},{9,8},{10,11... | collective-permute-start | bytes 1179656 | tf_op jit(solution)/shard_map/ppermute | solution.py:624
  25.3 0.2 collective-permute-start.9
  25.4 1.2 %shard_map.170.mine = f32[192,2048]{1,0:T(8,128)S(1)} custom-call(bf16[2,256,128]{2,1,0:T(8,128)(2,1)S(1)} %get-tuple-element.56.state, f32[8,512]{1,0:T(8,128)S(1)} %get-tuple-element.57.halo, f32[384,512]{1,0:T(8,128)S(1)} %get-tuple-element.51.refs_6_.raw, bf16[384,256]{1,0:T(8,128)(2,1)S(1)} %get-tuple-element.52.refs_7_.through, ...), custom_call_target="tpu_custom_call" | custom-call | flops 805306368 | bytes 1048576 | tf_op jit(solution)/shard_map/pallas_call | solution.py:32
  26.7 0.0 collective-permute-done.10.second
  26.7 0.5 %collective-permute-done.9.first = bf16[192,1024]{1,0:T(8,128)(2,1)S(1)} collective-permute-done((bf16[192,1024]{1,0:T(8,128)(2,1)S(1)}, bf16[192,1024]{1,0:T(8,128)(2,1)S(1)}, u32[]{:S(2)}, u32[]{:S(2)}) %collective-permute-start.9) | collective-permute-done | bytes 393248 | tf_op jit(solution)/shard_map/ppermute | solution.py:614
  27.2 0.9 %add_rows.1 = bf16[192,2048]{1,0:T(8,128)(2,1)} custom-call(f32[192,2048]{1,0:T(8,128)S(1)} %shard_map.170.mine, bf16[192,1024]{1,0:T(8,128)(2,1)S(1)} %collective-permute-done.9.first, bf16[192,1024]{1,0:T(8,128)(2,1)S(1)} %collective-permute-done.10.second), custom_call_target="tpu_custom_call" | custom-call | flops 1048576 | bytes 1048576 | tf_op jit(solution)/shard_map/add_rows/pallas_call | solution.py:628
  (8 shorter events, 0.0 us)
Async XLA Ops:
  0.0 3.8 %collective-permute-start = (bf16[384,1024]{1,0:T(8,128)(2,1)}, bf16[384,1024]{1,0:T(8,128)(2,1)S(1)}, u32[]{:S(2)}, u32[]{:S(2)}) collective-permute-start(bf16[384,1024]{1,0:T(8,128)(2,1)} %tok_hbm.1), channel_id=1, source_target_pairs={{0,1},{1,0},{2,3},{3,2},{4,5},{5,4},{6,7},{7,6},{8,9},{9,8},{10,11... | collective-permute-start | bytes 2359304 | tf_op jit(solution)/shard_map/ppermute | solution.py:475
  0.5 3.3 %copy-start.9 = (f32[2048]{0:T(1024)S(1)}, f32[2048]{0:T(1024)}, u32[]{:S(2)}) copy-start(f32[2048]{0:T(1024)} %param.18) | copy-start | bytes 24580
  0.5 3.3 %copy-start.10 = (f32[256]{0:T(256)S(1)}, f32[256]{0:T(256)}, u32[]{:S(2)}) copy-start(f32[256]{0:T(256)} %param.28) | copy-start | bytes 3076
  3.8 4.6 %copy-start.2 = (bf16[2048,512]{1,0:T(8,128)(2,1)S(1)}, bf16[2048,512]{1,0:T(8,128)(2,1)}, u32[]{:S(2)}) copy-start(bf16[2048,512]{1,0:T(8,128)(2,1)} %wc.3) | copy-start | bytes 6291460
  3.8 4.6 %copy-start.3 = (bf16[2048,512]{1,0:T(8,128)(2,1)S(1)}, bf16[2048,512]{1,0:T(8,128)(2,1)}, u32[]{:S(2)}) copy-start(bf16[2048,512]{1,0:T(8,128)(2,1)} %wh.1) | copy-start | bytes 6291460
  5.7 7.9 %collective-permute-start.3 = (bf16[72,256]{1,0:T(8,128)(2,1)S(1)}, bf16[72,256]{1,0:T(8,128)(2,1)S(1)}, u32[]{:S(2)}, u32[]{:S(2)}) collective-permute-start(bf16[72,256]{1,0:T(8,128)(2,1)S(1)} %get-tuple-element.38.send), channel_id=1, source_target_pairs={{0,5},{1,4},{2,7},{3,6},{4,1},{5,0},{6,3},{7,2},{8,13},{9,12},{10,... | collective-permute-start | bytes 110600 | tf_op jit(solution)/shard_map/ppermute | solution.py:571
  8.4 5.2 %collective-permute-start.1 = (bf16[72,256]{1,0:T(8,128)(2,1)S(1)}, bf16[72,256]{1,0:T(8,128)(2,1)S(1)}, u32[]{:S(2)}, u32[]{:S(2)}) collective-permute-start(bf16[72,256]{1,0:T(8,128)(2,1)S(1)} %get-tuple-element.38.send), channel_id=1, source_target_pairs={{0,1},{1,0},{2,3},{3,2},{4,5},{5,4},{6,7},{7,6},{8,9},{9,8},{10,11... | collective-permute-start | bytes 110600 | tf_op jit(solution)/shard_map/ppermute | solution.py:573
  8.4 3.6 %copy-start.4 = (bf16[2048,512]{1,0:T(8,128)(2,1)S(1)}, bf16[2048,512]{1,0:T(8,128)(2,1)}, u32[]{:S(2)}) copy-start(bf16[2048,512]{1,0:T(8,128)(2,1)} %wb.1) | copy-start | bytes 6291460
  8.4 3.6 %copy-start.6 = (bf16[2048,256]{1,0:T(8,128)(2,1)S(1)}, bf16[2048,256]{1,0:T(8,128)(2,1)}, u32[]{:S(2)}) copy-start(bf16[2048,256]{1,0:T(8,128)(2,1)} %wq.1) | copy-start | bytes 3145732
  8.4 3.6 %copy-start.8 = (bf16[3,512]{1,0:T(4,128)(2,1)S(1)}, bf16[3,512]{1,0:T(4,128)(2,1)}, u32[]{:S(2)}) copy-start(bf16[3,512]{1,0:T(4,128)(2,1)} %taps.3) | copy-start | bytes 9220
  10.3 4.3 %collective-permute-start.4 = (bf16[72,256]{1,0:T(8,128)(2,1)S(1)}, bf16[72,256]{1,0:T(8,128)(2,1)S(1)}, u32[]{:S(2)}, u32[]{:S(2)}) collective-permute-start(bf16[72,256]{1,0:T(8,128)(2,1)S(1)} %get-tuple-element.41), channel_id=1, source_target_pairs={{0,7},{1,6},{2,5},{3,4},{4,3},{5,2},{6,1},{7,0},{8,15},{9,14},{10,... | collective-permute-start | bytes 110600 | tf_op jit(solution)/shard_map/ppermute | solution.py:571
  11.9 3.6 %collective-permute-start.2 = (bf16[72,256]{1,0:T(8,128)(2,1)S(1)}, bf16[72,256]{1,0:T(8,128)(2,1)S(1)}, u32[]{:S(2)}, u32[]{:S(2)}) collective-permute-start(bf16[72,256]{1,0:T(8,128)(2,1)S(1)} %get-tuple-element.41), channel_id=1, source_target_pairs={{0,3},{1,2},{2,1},{3,0},{4,7},{5,6},{6,5},{7,4},{8,11},{9,10},{10,... | collective-permute-start | bytes 110600 | tf_op jit(solution)/shard_map/ppermute | solution.py:571
  12.1 7.8 %copy-start.5 = (bf16[2048,512]{1,0:T(8,128)(2,1)S(1)}, bf16[2048,512]{1,0:T(8,128)(2,1)}, u32[]{:S(2)}) copy-start(bf16[2048,512]{1,0:T(8,128)(2,1)} %wg.1) | copy-start | bytes 6291460
  12.1 7.8 %copy-start.7 = (f32[8,32,64]{2,1,0:T(8,128)S(1)}, f32[8,32,64]{2,1,0:T(8,128)}, u32[]{:S(2)}) copy-start(f32[8,32,64]{2,1,0:T(8,128)} %param.30) | copy-start | bytes 196612
  12.1 7.8 %copy-start.11 = (f32[64]{0:T(128)S(1)}, f32[64]{0:T(128)}, u32[]{:S(2)}) copy-start(f32[64]{0:T(128)} %param.31) | copy-start | bytes 772
  15.6 6.7 %collective-permute-start.7 = (bf16[72,256]{1,0:T(8,128)(2,1)S(1)}, bf16[72,256]{1,0:T(8,128)(2,1)S(1)}, u32[]{:S(2)}, u32[]{:S(2)}) collective-permute-start(bf16[72,256]{1,0:T(8,128)(2,1)S(1)} %get-tuple-element.42.refs_0_), channel_id=1, source_target_pairs={{0,25},{1,24},{2,27},{3,26},{4,29},{5,28},{6,31},{7,30},{8,17},{9,... | collective-permute-start | bytes 110600 | tf_op jit(solution)/shard_map/ppermute | solution.py:571
  19.0 4.4 %collective-permute-start.6 = (bf16[72,256]{1,0:T(8,128)(2,1)S(1)}, bf16[72,256]{1,0:T(8,128)(2,1)S(1)}, u32[]{:S(2)}, u32[]{:S(2)}) collective-permute-start(bf16[72,256]{1,0:T(8,128)(2,1)S(1)} %get-tuple-element.42.refs_0_), channel_id=1, source_target_pairs={{0,17},{1,16},{2,19},{3,18},{4,21},{5,20},{6,23},{7,22},{8,25},{9,... | collective-permute-start | bytes 110600 | tf_op jit(solution)/shard_map/ppermute | solution.py:571
  19.0 4.4 %collective-permute-start.5 = (bf16[72,256]{1,0:T(8,128)(2,1)S(1)}, bf16[72,256]{1,0:T(8,128)(2,1)S(1)}, u32[]{:S(2)}, u32[]{:S(2)}) collective-permute-start(bf16[72,256]{1,0:T(8,128)(2,1)S(1)} %get-tuple-element.42.refs_0_), channel_id=1, source_target_pairs={{0,9},{1,8},{2,11},{3,10},{4,13},{5,12},{6,15},{7,14},{8,1},{9,0},... | collective-permute-start | bytes 110600 | tf_op jit(solution)/shard_map/ppermute | solution.py:571
  19.6 2.7 %collective-permute-start.8 = (bf16[72,256]{1,0:T(8,128)(2,1)S(1)}, bf16[72,256]{1,0:T(8,128)(2,1)S(1)}, u32[]{:S(2)}, u32[]{:S(2)}) collective-permute-start(bf16[72,256]{1,0:T(8,128)(2,1)S(1)} %get-tuple-element.43), channel_id=1, source_target_pairs={{0,1},{1,0},{2,3},{3,2},{4,5},{5,4},{6,7},{7,6},{8,9},{9,8},{10,11... | collective-permute-start | bytes 110600 | tf_op jit(solution)/shard_map/ppermute | solution.py:575
  19.9 3.5 %copy-start = (bf16[512,2048]{1,0:T(8,128)(2,1)S(1)}, bf16[512,2048]{1,0:T(8,128)(2,1)}, u32[]{:S(2)}) copy-start(bf16[512,2048]{1,0:T(8,128)(2,1)} %wc.5) | copy-start | bytes 6291460
  19.9 3.5 %copy-start.1 = (bf16[512,2048]{1,0:T(8,128)(2,1)S(1)}, bf16[512,2048]{1,0:T(8,128)(2,1)}, u32[]{:S(2)}) copy-start(bf16[512,2048]{1,0:T(8,128)(2,1)} %wa.3) | copy-start | bytes 6291460
  24.9 1.8 %collective-permute-start.10 = (bf16[192,1024]{1,0:T(8,128)(2,1)S(1)}, bf16[192,1024]{1,0:T(8,128)(2,1)S(1)}, u32[]{:S(2)}, u32[]{:S(2)}) collective-permute-start(bf16[192,1024]{1,0:T(8,128)(2,1)S(1)} %shard_map.171), channel_id=1, source_target_pairs={{0,1},{1,0},{2,3},{3,2},{4,5},{5,4},{6,7},{7,6},{8,9},{9,8},{10,11... | collective-permute-start | bytes 1179656 | tf_op jit(solution)/shard_map/ppermute | solution.py:624
  25.3 2.0 %collective-permute-start.9 = (bf16[192,1024]{1,0:T(8,128)(2,1)S(1)}, bf16[192,1024]{1,0:T(8,128)(2,1)S(1)}, u32[]{:S(2)}, u32[]{:S(2)}) collective-permute-start(bf16[192,1024]{1,0:T(8,128)(2,1)S(1)} %get-tuple-element.58), channel_id=1, source_target_pairs={{0,1},{1,0},{2,3},{3,2},{4,5},{5,4},{6,7},{7,6},{8,9},{9,8},{10,11... | collective-permute-start | bytes 1179656 | tf_op jit(solution)/shard_map/ppermute | solution.py:614
where the time goes:
time: 28.3 us; the launch traced here: 28.2 us
  Pallas kernels  14.6 us (52%)
  starting transfers between devices  9.79 us (35%)
  waiting for transfers between devices  3.44 us (12%)
    pallas_call x9, Pallas kernels, call(): pl.pallas_call(body, out_shape=[jax.ShapeDtypeStruct(s, d) for s, d in ou...  13.7 us
    ppermute x6, starting transfers between devices, on_device(): items[j] = lax.ppermute(payload, ('sp', 'tp'), pairs)  8.47 us
    ppermute x6, waiting for transfers between devices, on_device(): items[j] = lax.ppermute(payload, ('sp', 'tp'), pairs)  2.91 us
    pallas_call x1, Pallas kernels, on_device(): pl.pallas_call(add_rows, out_shape=jax.ShapeDtypeStruct((rows // 2, model...  0.94 us
  transfers between devices with their start and end apart: 11, of which 4 were waited for; matrix products, arithmetic and copies ran while one was open for 0% of the time, Pallas kernels for 36%

commit v1 on v0

--- a/solution.py
+++ b/solution.py
@@ -266,17 +266,27 @@
     return (s * tile_lanes(r, s.shape[1])).astype(BF16)
 
 
-def conv_inputs(full, scale, wc, wh, send, prod, out):
-    r = scale[...]
-    x = full[...]
+def conv_product(full, scale, wc, wh, rows):
+    r = scale[rows, :]
+    x = full[rows, :]
     p = scaled(x, wc[...], r).astype(F32) * scaled(x, wh[...], r).astype(F32)
-    p = p.astype(BF16)
-    prod[...] = p
+    return p.astype(BF16)
+
+
+def conv_halo(full, scale, wc, wh, send, out):
+    rows = full.shape[0]
+    p = conv_product(full, scale, wc, wh, slice(rows - 16, rows))
     dv = send.shape[0] - EXTRA_ROWS
-    tail = to_tail(p[p.shape[0] - 16 :].astype(F32))
+    tail = to_tail(p.astype(F32))
     row = lax.broadcasted_iota(jnp.int32, tail.shape, 0)
     out[:dv, :] = send[:dv, :]
     out[dv:, :] = jnp.where(row < 2, send[dv:, :].astype(F32), tail).astype(BF16)
+
+
+def conv_inputs(full, scale, wc, wh, wg, gain, prod, gate):
+    prod[...] = conv_product(full, scale, wc, wh, slice(0, full.shape[0]))
+    gated = scaled(full[...], wg[...], scale[...]).astype(F32)
+    gate[...] = gated * jax.nn.sigmoid(gated) * tile_lanes(gain[...], gated.shape[1])
 
 
 def late_half(full, scale, taps, wb, wq, prod, query, outer, conv):
@@ -297,14 +307,12 @@
 
 
 def blockwise(
-    key_dim, query, key, val, cum, base, start, full, scale, wg, gain, raw, through, first, gate
+    key_dim, query, key, val, cum, base, start, raw, through, first
 ):
     rows = query.shape[0]
     n = rows // BLOCK
     shrink = key_dim**-0.5
     first[...] = start[...].T
-    gated = scaled(full[...], wg[...], scale[...]).astype(F32)
-    gate[...] = gated * jax.nn.sigmoid(gated) * tile_lanes(gain[...], gated.shape[1])
     k_mask = block_mask(256, 64, 128, 32)
     v_mask = block_mask(256, 64, 256, 64)
     causal = lax.broadcasted_iota(jnp.int32, (BLOCK, 256), 0) >= (
@@ -513,11 +521,27 @@
         + [(a, VMEM) for a in (acc, xg, ssq, wide, ahead)],
         flops,
     )
-    prod, send_halo = call(
+    (send_halo,) = call(
+        conv_halo,
+        [(send.shape, BF16)],
+        [(a, VMEM) for a in (full, scale, inner_gate_weight, convolution_input_weight, send)],
+        2 * rows * half * cw,
+    )
+    prod, gate = call(
         conv_inputs,
-        [((rows, cw), BF16), (send.shape, BF16)],
-        [(a, VMEM) for a in (full, scale, inner_gate_weight, convolution_input_weight, send)],
-        2 * rows * 2 * half * 2 * cw,
+        [((rows, cw), BF16), ((rows, vw), F32)],
+        [
+            (a, VMEM)
+            for a in (
+                full,
+                scale,
+                inner_gate_weight,
+                convolution_input_weight,
+                attention_gate_weight,
+                head_norm_gain.reshape(1, -1),
+            )
+        ],
+        2 * rows * 2 * half * (2 * cw + vw),
     )
     query, outer, conv = call(
         late_half,
@@ -535,25 +559,14 @@
         ],
         2 * rows * 2 * half * (kw + cw),
     )
-    raw, through, first, gate = call(
+    raw, through, first = call(
         functools.partial(blockwise, dk),
-        [((rows, vw), F32), ((rows, kw), BF16), ((dv, kw), F32), ((rows, vw), F32)],
+        [((rows, vw), F32), ((rows, kw), BF16), ((dv, kw), F32)],
         [
             (a, VMEM)
-            for a in (
-                query,
-                key,
-                val,
-                cum,
-                base,
-                initial_head_state.reshape(heads * dk, dv),
-                full,
-                scale,
-                attention_gate_weight,
-                head_norm_gain.reshape(1, -1),
-            )
-        ],
-        2 * rows * 2 * half * (kw + vw),
+            for a in (query, key, val, cum, base, initial_head_state.reshape(heads * dk, dv))
+        ],
+        1 << 24,
     )
     pre = ()
     stride = 1

time: 28.3 us -> 27.2 us (0.961)
  waiting for transfers between devices: 3.44 us -> 1.18 us
  Pallas kernels: 14.6 us -> 15.4 us
  local copies, waits for them, and re-layouts: 0.06 us -> 0.35 us
    ppermute x6, waiting for transfers between devices: 2.91 us -> 0.66 us  [on_device(): items[j] = lax.ppermute(payload, ('sp', 'tp'), pairs)]
    pallas_call x9 -> x10, Pallas kernels: 13.7 us -> 14.4 us  [call(): pl.pallas_call(body, out_shape=[jax.ShapeDtypeStruct(s, d) for s, d in ou...]
    ppermute x1, starting transfers between devices: 0.01 us -> 0.51 us  [on_device(): items[0] = lax.ppermute(send, 'tp', swap)]
    ppermute x6, starting transfers between devices: 8.47 us -> 8.07 us  [on_device(): items[j] = lax.ppermute(payload, ('sp', 'tp'), pairs)]
  transfers between devices with their start and end apart: 11 -> 11, of which waited for: 4 -> 2; matrix products, arithmetic and copies ran while one was open for 0% -> 0% of each run, Pallas kernels for 36% -> 38%
where the time goes in v1:
time: 27.2 us; the launch traced here: 27.1 us
  Pallas kernels  15.4 us (57%)
  starting transfers between devices  9.98 us (37%)
  waiting for transfers between devices  1.18 us (4%)
  local copies, waits for them, and re-layouts  0.35 us (1%)
    pallas_call x10, Pallas kernels, call(): pl.pallas_call(body, out_shape=[jax.ShapeDtypeStruct(s, d) for s, d in ou...  14.4 us
    ppermute x6, starting transfers between devices, on_device(): items[j] = lax.ppermute(payload, ('sp', 'tp'), pairs)  8.07 us
    pallas_call x1, Pallas kernels, on_device(): pl.pallas_call(add_rows, out_shape=jax.ShapeDtypeStruct((rows // 2, model...  0.95 us
    ppermute x6, waiting for transfers between devices, on_device(): items[j] = lax.ppermute(payload, ('sp', 'tp'), pairs)  0.66 us
  transfers between devices with their start and end apart: 11, of which 2 were waited for; matrix products, arithmetic and copies ran while one was open for 0% of the time, Pallas kernels for 38%

profile of v1, /device:TPU:0, one launch (start us, length us, event | category | flops | bytes accessed | tf_op | source)
XLA Modules:
  0.0 27.1 jit_solution(14622705301282714876)
XLA Ops:
  0.0 0.5 %collective-permute-start = (bf16[384,1024]{1,0:T(8,128)(2,1)}, bf16[384,1024]{1,0:T(8,128)(2,1)S(1)}, u32[]{:S(2)}, u32[]{:S(2)}) collective-permute-start(bf16[384,1024]{1,0:T(8,128)(2,1)} %tok_hbm.1), channel_id=1, source_target_pairs={{0,1},{1,0},{2,3},{3,2},{4,5},{5,4},{6,7},{7,6},{8,9},{9,8},{10,11... | collective-permute-start | bytes 2359304 | tf_op jit(solution)/shard_map/ppermute | solution.py:483
  0.5 3.3 %shard_map.163 = (f32[384,1024]{1,0:T(8,128)S(1)}, bf16[384,1024]{1,0:T(8,128)(2,1)S(1)}, f32[384,128]{1,0:T(8,128)S(1)}, f32[384,256]{1,0:T(8,128)S(1)}, bf16[1024,1024]{1,0:T(8,128)(2,1)S(1)}) custom-call(bf16[384,1024]{1,0:T(8,128)(2,1)} %tok_hbm.1, f32[1,2048]{1,0:T(1,128)} %bitcast.6, f32[8,384]{1,0:T(8,128)} %bitcast.10, bf16[2048,256]{1,0:T(8,128)(2,1)} %refs_0_.1, ...), custom_call_target="tpu_custom_call" | custom-call | flops 805306368 | bytes 1048576 | tf_op jit(solution)/shard_map/pallas_call | solution.py:32
  3.8 0.0 collective-permute-done.tok
  3.8 0.0 copy-done.8
  3.8 0.0 copy-done.9
  3.8 0.0 copy-start.2
  3.8 0.0 copy-start.3
  3.8 1.9 %shard_map.164 = (bf16[384,2048]{1,0:T(8,128)(2,1)S(1)}, f32[384,128]{1,0:T(8,128)S(1)}, bf16[384,256]{1,0:T(8,128)(2,1)S(1)}, bf16[384,512]{1,0:T(8,128)(2,1)S(...) custom-call(bf16[384,1024]{1,0:T(8,128)(2,1)S(1)} %collective-permute-done.tok, ...), custom_call_target="tpu_custom_call" | custom-call | flops 805306368 | bytes 1048576 | tf_op jit(solution)/shard_map/pallas_call | solution.py:32
  5.7 0.0 copy-done.2
  5.7 0.3 %copy-done.3 = bf16[2048,512]{1,0:T(8,128)(2,1)S(1)} copy-done((bf16[2048,512]{1,0:T(8,128)(2,1)S(1)}, bf16[2048,512]{1,0:T(8,128)(2,1)}, u32[]{:S(2)}) %copy-start.3) | copy-done | bytes 2097176
  6.0 0.7 %shard_map.165 = bf16[72,256]{1,0:T(8,128)(2,1)S(1)} custom-call(bf16[384,2048]{1,0:T(8,128)(2,1)S(1)} %get-tuple-element.38.full, f32[384,128]{1,0:T(8,128)S(1)} %get-tuple-element.39.scale, bf16[2048,512]{1,0:T(8,128)(2,1)S(1)} %copy-done.2, bf16[2048,512]{1,0:T(8,128)(2,1)S(1)} %copy-done.3, bf16[72,256]{1,0:T(8,128)(2,1)S(1)} %get-tuple-element.37.send), custom_call_target="tpu_custom_call" | custom-call | flops 402653184 | bytes 1048576 | tf_op jit(solution)/shard_map/pallas_call | solution.py:32
  6.7 3.6 %collective-permute-start.4 = (bf16[72,256]{1,0:T(8,128)(2,1)S(1)}, bf16[72,256]{1,0:T(8,128)(2,1)S(1)}, u32[]{:S(2)}, u32[]{:S(2)}) collective-permute-start(bf16[72,256]{1,0:T(8,128)(2,1)S(1)} %shard_map.165), channel_id=1, source_target_pairs={{0,7},{1,6},{2,5},{3,4},{4,3},{5,2},{6,1},{7,0},{8,15},{9,14},{10,... | collective-permute-start | bytes 110600 | tf_op jit(solution)/shard_map/ppermute | solution.py:584
  10.3 0.1 collective-permute-start.2
  10.5 0.1 collective-permute-start.3
  10.6 0.5 %collective-permute-start.1 = (bf16[72,256]{1,0:T(8,128)(2,1)S(1)}, bf16[72,256]{1,0:T(8,128)(2,1)S(1)}, u32[]{:S(2)}, u32[]{:S(2)}) collective-permute-start(bf16[72,256]{1,0:T(8,128)(2,1)S(1)} %get-tuple-element.37.send), channel_id=1, source_target_pairs={{0,1},{1,0},{2,3},{3,2},{4,5},{5,4},{6,7},{7,6},{8,9},{9,8},{10,11... | collective-permute-start | bytes 110600 | tf_op jit(solution)/shard_map/ppermute | solution.py:586
  11.1 0.0 copy-done.10
  11.1 0.0 copy-done.11
  11.1 0.0 copy-start.7
  11.1 2.8 %shard_map.167 = (bf16[384,512]{1,0:T(8,128)(2,1)S(1)}, f32[384,512]{1,0:T(8,128)S(1)}) custom-call(bf16[384,2048]{1,0:T(8,128)(2,1)S(1)} %get-tuple-element.38.full, f32[384,128]{1,0:T(8,128)S(1)} %get-tuple-element.39.scale, bf16[2048,512]{1,0:T(8,128)(2,1)S(1)} %copy-done.2, bf16[2048,512]{1,0:T(8,128)(2,1)S(1)} %copy-done.3, ...), custom_call_target="tpu_custom_call" | custom-call | flops 2415919104 | bytes 1048576 | tf_op jit(solution)/shard_map/pallas_call | solution.py:32
  13.9 0.0 collective-permute-done.4.refs_3_
  13.9 0.0 collective-permute-done.2.refs_1_
  13.9 0.0 collective-permute-done.3.refs_2_
  13.9 0.0 collective-permute-done.1.refs_0_
  13.9 0.1 shard_map.166
  14.0 3.8 %collective-permute-start.7 = (bf16[72,256]{1,0:T(8,128)(2,1)S(1)}, bf16[72,256]{1,0:T(8,128)(2,1)S(1)}, u32[]{:S(2)}, u32[]{:S(2)}) collective-permute-start(bf16[72,256]{1,0:T(8,128)(2,1)S(1)} %get-tuple-element.40.refs_0_), channel_id=1, source_target_pairs={{0,25},{1,24},{2,27},{3,26},{4,29},{5,28},{6,31},{7,30},{8,17},{9,... | collective-permute-start | bytes 110600 | tf_op jit(solution)/shard_map/ppermute | solution.py:584
  17.8 0.0 collective-permute-start.6
  17.8 0.4 %collective-permute-start.5 = (bf16[72,256]{1,0:T(8,128)(2,1)S(1)}, bf16[72,256]{1,0:T(8,128)(2,1)S(1)}, u32[]{:S(2)}, u32[]{:S(2)}) collective-permute-start(bf16[72,256]{1,0:T(8,128)(2,1)S(1)} %get-tuple-element.40.refs_0_), channel_id=1, source_target_pairs={{0,9},{1,8},{2,11},{3,10},{4,13},{5,12},{6,15},{7,14},{8,1},{9,0},... | collective-permute-start | bytes 110600 | tf_op jit(solution)/shard_map/ppermute | solution.py:584
  18.2 0.3 %collective-permute-start.8 = (bf16[72,256]{1,0:T(8,128)(2,1)S(1)}, bf16[72,256]{1,0:T(8,128)(2,1)S(1)}, u32[]{:S(2)}, u32[]{:S(2)}) collective-permute-start(bf16[72,256]{1,0:T(8,128)(2,1)S(1)} %get-tuple-element.41), channel_id=1, source_target_pairs={{0,1},{1,0},{2,3},{3,2},{4,5},{5,4},{6,7},{7,6},{8,9},{9,8},{10,11... | collective-permute-start | bytes 110600 | tf_op jit(solution)/shard_map/ppermute | solution.py:588
  18.5 0.0 copy-done.4
  18.5 0.0 copy-done.5
  18.5 0.0 copy-done.7
  18.6 0.0 copy-start
  18.6 0.0 copy-start.1
  18.6 1.5 %shard_map.168 = (bf16[384,256]{1,0:T(8,128)(2,1)S(1)}, bf16[384,512]{1,0:T(8,128)(2,1)S(1)}, bf16[384,512]{1,0:T(8,128)(2,1)S(1)}) custom-call(bf16[384,2048]{1,0:T(8,128)(2,1)S(1)} %get-tuple-element.38.full, f32[384,128]{1,0:T(8,128)S(1)} %get-tuple-element.39.scale, bf16[3,512]{1,0:T(4,128)(2,1)S(1)} %copy-done.7, bf16[2048,512]{1,0:T(8,128)(2,1)S(1)} %copy-done.4, ...), custom_call_target="tpu_custom_call" | custom-call | flops 1207959552 | bytes 1048576 | tf_op jit(solution)/shard_map/pallas_call | solution.py:32
  20.1 1.5 %shard_map.169 = (f32[384,512]{1,0:T(8,128)S(1)}, bf16[384,256]{1,0:T(8,128)(2,1)S(1)}, f32[64,256]{1,0:T(8,128)S(1)}) custom-call(bf16[384,256]{1,0:T(8,128)(2,1)S(1)} %get-tuple-element.43.query, bf16[384,256]{1,0:T(8,128)(2,1)S(1)} %get-tuple-element.44.key, bf16[384,512]{1,0:T(8,128)(2,1)S(1)} %get-tuple-element.45.val, ...), custom_call_target="tpu_custom_call" | custom-call | flops 16777216 | bytes 1048576 | tf_op jit(solution)/shard_map/pallas_call | solution.py:32
  21.6 0.0 collective-permute-done.8.refs_4_
  21.6 0.0 collective-permute-done.7.refs_3_
  21.6 0.6 %collective-permute-done.6.refs_2_ = bf16[72,256]{1,0:T(8,128)(2,1)S(1)} collective-permute-done((bf16[72,256]{1,0:T(8,128)(2,1)S(1)}, bf16[72,256]{1,0:T(8,128)(2,1)S(1)}, u32[]{:S(2)}, u32[]{:S(2)}) %collective-permute-start.6) | collective-permute-done | bytes 36896 | tf_op jit(solution)/shard_map/ppermute | solution.py:584
  22.3 0.0 collective-permute-done.5.refs_1_
  22.3 0.0 copy-done.1
  22.3 0.9 %shard_map.170 = (bf16[192,1024]{1,0:T(8,128)(2,1)S(1)}, bf16[192,512]{1,0:T(8,128)(2,1)S(1)}, bf16[192,512]{1,0:T(8,128)(2,1)S(1)}, bf16[2,256,128]{2,1,0:T(8,128)(2,1)S(1)}, f32[8,512]{1,0:T(8,128)S(1)}) custom-call(bf16[72,256]{1,0:T(8,128)(2,1)S(1)} %get-tuple-element.40.refs_0_, bf16[72,256]{1,0:T(8,128)(2,1)S(1)} %collective-permute-done.5.refs_1_, ...), custom_call_target="tpu_custom_call" | custom-call | flops 402653184 | bytes 1048576 | tf_op jit(solution)/shard_map/pallas_call | solution.py:32
  23.2 0.6 %shard_map.172 = bf16[192,1024]{1,0:T(8,128)(2,1)S(1)} custom-call(bf16[192,512]{1,0:T(8,128)(2,1)S(1)} %get-tuple-element.57.left, bf16[192,512]{1,0:T(8,128)(2,1)S(1)} %get-tuple-element.58.attn, bf16[512,2048]{1,0:T(8,128)(2,1)S(1)} %copy-done, bf16[512,2048]{1,0:T(8,128)(2,1)S(1)} %copy-done.1), custom_call_target="tpu_custom_call" | custom-call | flops 402653184 | bytes 1048576 | tf_op jit(solution)/shard_map/pallas_call | solution.py:32
  23.8 0.2 collective-permute-start.10
  24.0 0.4 %collective-permute-start.9 = (bf16[192,1024]{1,0:T(8,128)(2,1)S(1)}, bf16[192,1024]{1,0:T(8,128)(2,1)S(1)}, u32[]{:S(2)}, u32[]{:S(2)}) collective-permute-start(bf16[192,1024]{1,0:T(8,128)(2,1)S(1)} %get-tuple-element.56), channel_id=1, source_target_pairs={{0,1},{1,0},{2,3},{3,2},{4,5},{5,4},{6,7},{7,6},{8,9},{9,8},{10,11... | collective-permute-start | bytes 1179656 | tf_op jit(solution)/shard_map/ppermute | solution.py:627
  24.4 1.2 %shard_map.171.mine = f32[192,2048]{1,0:T(8,128)S(1)} custom-call(bf16[2,256,128]{2,1,0:T(8,128)(2,1)S(1)} %get-tuple-element.54.state, f32[8,512]{1,0:T(8,128)S(1)} %get-tuple-element.55.halo, f32[384,512]{1,0:T(8,128)S(1)} %get-tuple-element.49.refs_6_.raw, bf16[384,256]{1,0:T(8,128)(2,1)S(1)} %get-tuple-element.50.refs_7_.through, ...), custom_call_target="tpu_custom_call" | custom-call | flops 805306368 | bytes 1048576 | tf_op jit(solution)/shard_map/pallas_call | solution.py:32
  25.6 0.0 collective-permute-done.10.second
  25.6 0.5 %collective-permute-done.9.first = bf16[192,1024]{1,0:T(8,128)(2,1)S(1)} collective-permute-done((bf16[192,1024]{1,0:T(8,128)(2,1)S(1)}, bf16[192,1024]{1,0:T(8,128)(2,1)S(1)}, u32[]{:S(2)}, u32[]{:S(2)}) %collective-permute-start.9) | collective-permute-done | bytes 393248 | tf_op jit(solution)/shard_map/ppermute | solution.py:627
  26.1 0.9 %add_rows.1 = bf16[192,2048]{1,0:T(8,128)(2,1)} custom-call(f32[192,2048]{1,0:T(8,128)S(1)} %shard_map.171.mine, bf16[192,1024]{1,0:T(8,128)(2,1)S(1)} %collective-permute-done.9.first, bf16[192,1024]{1,0:T(8,128)(2,1)S(1)} %collective-permute-done.10.second), custom_call_target="tpu_custom_call" | custom-call | flops 1048576 | bytes 1048576 | tf_op jit(solution)/shard_map/add_rows/pallas_call | solution.py:641
  (9 shorter events, 0.0 us)
Async XLA Ops:
  0.0 3.8 %collective-permute-start = (bf16[384,1024]{1,0:T(8,128)(2,1)}, bf16[384,1024]{1,0:T(8,128)(2,1)S(1)}, u32[]{:S(2)}, u32[]{:S(2)}) collective-permute-start(bf16[384,1024]{1,0:T(8,128)(2,1)} %tok_hbm.1), channel_id=1, source_target_pairs={{0,1},{1,0},{2,3},{3,2},{4,5},{5,4},{6,7},{7,6},{8,9},{9,8},{10,11... | collective-permute-start | bytes 2359304 | tf_op jit(solution)/shard_map/ppermute | solution.py:483
  0.5 3.3 %copy-start.8 = (f32[2048]{0:T(1024)S(1)}, f32[2048]{0:T(1024)}, u32[]{:S(2)}) copy-start(f32[2048]{0:T(1024)} %param.18) | copy-start | bytes 24580
  0.5 3.3 %copy-start.9 = (f32[256]{0:T(256)S(1)}, f32[256]{0:T(256)}, u32[]{:S(2)}) copy-start(f32[256]{0:T(256)} %param.28) | copy-start | bytes 3076
  3.8 1.9 %copy-start.2 = (bf16[2048,512]{1,0:T(8,128)(2,1)S(1)}, bf16[2048,512]{1,0:T(8,128)(2,1)}, u32[]{:S(2)}) copy-start(bf16[2048,512]{1,0:T(8,128)(2,1)} %wc.5) | copy-start | bytes 6291460
  3.8 2.2 %copy-start.3 = (bf16[2048,512]{1,0:T(8,128)(2,1)S(1)}, bf16[2048,512]{1,0:T(8,128)(2,1)}, u32[]{:S(2)}) copy-start(bf16[2048,512]{1,0:T(8,128)(2,1)} %wh.3) | copy-start | bytes 6291460
  6.0 5.1 %copy-start.10 = (bf16[2048,512]{1,0:T(8,128)(2,1)S(1)}, bf16[2048,512]{1,0:T(8,128)(2,1)}, u32[]{:S(2)}) copy-start(bf16[2048,512]{1,0:T(8,128)(2,1)} %wg.1) | copy-start | bytes 6291460
  6.0 5.1 %copy-start.11 = (f32[64]{0:T(128)S(1)}, f32[64]{0:T(128)}, u32[]{:S(2)}) copy-start(f32[64]{0:T(128)} %param.31) | copy-start | bytes 772
  6.7 7.2 %collective-permute-start.4 = (bf16[72,256]{1,0:T(8,128)(2,1)S(1)}, bf16[72,256]{1,0:T(8,128)(2,1)S(1)}, u32[]{:S(2)}, u32[]{:S(2)}) collective-permute-start(bf16[72,256]{1,0:T(8,128)(2,1)S(1)} %shard_map.165), channel_id=1, source_target_pairs={{0,7},{1,6},{2,5},{3,4},{4,3},{5,2},{6,1},{7,0},{8,15},{9,14},{10,... | collective-permute-start | bytes 110600 | tf_op jit(solution)/shard_map/ppermute | solution.py:584
  10.3 3.6 %collective-permute-start.2 = (bf16[72,256]{1,0:T(8,128)(2,1)S(1)}, bf16[72,256]{1,0:T(8,128)(2,1)S(1)}, u32[]{:S(2)}, u32[]{:S(2)}) collective-permute-start(bf16[72,256]{1,0:T(8,128)(2,1)S(1)} %shard_map.165), channel_id=1, source_target_pairs={{0,3},{1,2},{2,1},{3,0},{4,7},{5,6},{6,5},{7,4},{8,11},{9,10},{10,... | collective-permute-start | bytes 110600 | tf_op jit(solution)/shard_map/ppermute | solution.py:584
  10.5 3.5 %collective-permute-start.3 = (bf16[72,256]{1,0:T(8,128)(2,1)S(1)}, bf16[72,256]{1,0:T(8,128)(2,1)S(1)}, u32[]{:S(2)}, u32[]{:S(2)}) collective-permute-start(bf16[72,256]{1,0:T(8,128)(2,1)S(1)} %get-tuple-element.37.send), channel_id=1, source_target_pairs={{0,5},{1,4},{2,7},{3,6},{4,1},{5,0},{6,3},{7,2},{8,13},{9,12},{10,... | collective-permute-start | bytes 110600 | tf_op jit(solution)/shard_map/ppermute | solution.py:584
  10.6 3.3 %collective-permute-start.1 = (bf16[72,256]{1,0:T(8,128)(2,1)S(1)}, bf16[72,256]{1,0:T(8,128)(2,1)S(1)}, u32[]{:S(2)}, u32[]{:S(2)}) collective-permute-start(bf16[72,256]{1,0:T(8,128)(2,1)S(1)} %get-tuple-element.37.send), channel_id=1, source_target_pairs={{0,1},{1,0},{2,3},{3,2},{4,5},{5,4},{6,7},{7,6},{8,9},{9,8},{10,11... | collective-permute-start | bytes 110600 | tf_op jit(solution)/shard_map/ppermute | solution.py:586
  11.1 7.5 %copy-start.4 = (bf16[2048,512]{1,0:T(8,128)(2,1)S(1)}, bf16[2048,512]{1,0:T(8,128)(2,1)}, u32[]{:S(2)}) copy-start(bf16[2048,512]{1,0:T(8,128)(2,1)} %wb.1) | copy-start | bytes 6291460
  11.1 7.5 %copy-start.5 = (bf16[2048,256]{1,0:T(8,128)(2,1)S(1)}, bf16[2048,256]{1,0:T(8,128)(2,1)}, u32[]{:S(2)}) copy-start(bf16[2048,256]{1,0:T(8,128)(2,1)} %wq.1) | copy-start | bytes 3145732
  11.1 7.5 %copy-start.7 = (bf16[3,512]{1,0:T(4,128)(2,1)S(1)}, bf16[3,512]{1,0:T(4,128)(2,1)}, u32[]{:S(2)}) copy-start(bf16[3,512]{1,0:T(4,128)(2,1)} %taps.3) | copy-start | bytes 9220
  14.0 7.6 %collective-permute-start.7 = (bf16[72,256]{1,0:T(8,128)(2,1)S(1)}, bf16[72,256]{1,0:T(8,128)(2,1)S(1)}, u32[]{:S(2)}, u32[]{:S(2)}) collective-permute-start(bf16[72,256]{1,0:T(8,128)(2,1)S(1)} %get-tuple-element.40.refs_0_), channel_id=1, source_target_pairs={{0,25},{1,24},{2,27},{3,26},{4,29},{5,28},{6,31},{7,30},{8,17},{9,... | collective-permute-start | bytes 110600 | tf_op jit(solution)/shard_map/ppermute | solution.py:584
  17.8 4.5 %collective-permute-start.6 = (bf16[72,256]{1,0:T(8,128)(2,1)S(1)}, bf16[72,256]{1,0:T(8,128)(2,1)S(1)}, u32[]{:S(2)}, u32[]{:S(2)}) collective-permute-start(bf16[72,256]{1,0:T(8,128)(2,1)S(1)} %get-tuple-element.40.refs_0_), channel_id=1, source_target_pairs={{0,17},{1,16},{2,19},{3,18},{4,21},{5,20},{6,23},{7,22},{8,25},{9,... | collective-permute-start | bytes 110600 | tf_op jit(solution)/shard_map/ppermute | solution.py:584
  17.8 4.5 %collective-permute-start.5 = (bf16[72,256]{1,0:T(8,128)(2,1)S(1)}, bf16[72,256]{1,0:T(8,128)(2,1)S(1)}, u32[]{:S(2)}, u32[]{:S(2)}) collective-permute-start(bf16[72,256]{1,0:T(8,128)(2,1)S(1)} %get-tuple-element.40.refs_0_), channel_id=1, source_target_pairs={{0,9},{1,8},{2,11},{3,10},{4,13},{5,12},{6,15},{7,14},{8,1},{9,0},... | collective-permute-start | bytes 110600 | tf_op jit(solution)/shard_map/ppermute | solution.py:584
  18.2 3.4 %collective-permute-start.8 = (bf16[72,256]{1,0:T(8,128)(2,1)S(1)}, bf16[72,256]{1,0:T(8,128)(2,1)S(1)}, u32[]{:S(2)}, u32[]{:S(2)}) collective-permute-start(bf16[72,256]{1,0:T(8,128)(2,1)S(1)} %get-tuple-element.41), channel_id=1, source_target_pairs={{0,1},{1,0},{2,3},{3,2},{4,5},{5,4},{6,7},{7,6},{8,9},{9,8},{10,11... | collective-permute-start | bytes 110600 | tf_op jit(solution)/shard_map/ppermute | solution.py:588
  18.5 1.5 %copy-start.6 = (f32[8,32,64]{2,1,0:T(8,128)S(1)}, f32[8,32,64]{2,1,0:T(8,128)}, u32[]{:S(2)}) copy-start(f32[8,32,64]{2,1,0:T(8,128)} %param.30) | copy-start | bytes 196612
  18.6 3.7 %copy-start = (bf16[512,2048]{1,0:T(8,128)(2,1)S(1)}, bf16[512,2048]{1,0:T(8,128)(2,1)}, u32[]{:S(2)}) copy-start(bf16[512,2048]{1,0:T(8,128)(2,1)} %wc.7) | copy-start | bytes 6291460
  18.6 3.7 %copy-start.1 = (bf16[512,2048]{1,0:T(8,128)(2,1)S(1)}, bf16[512,2048]{1,0:T(8,128)(2,1)}, u32[]{:S(2)}) copy-start(bf16[512,2048]{1,0:T(8,128)(2,1)} %wa.3) | copy-start | bytes 6291460
  23.8 1.8 %collective-permute-start.10 = (bf16[192,1024]{1,0:T(8,128)(2,1)S(1)}, bf16[192,1024]{1,0:T(8,128)(2,1)S(1)}, u32[]{:S(2)}, u32[]{:S(2)}) collective-permute-start(bf16[192,1024]{1,0:T(8,128)(2,1)S(1)} %shard_map.172), channel_id=1, source_target_pairs={{0,1},{1,0},{2,3},{3,2},{4,5},{5,4},{6,7},{7,6},{8,9},{9,8},{10,11... | collective-permute-start | bytes 1179656 | tf_op jit(solution)/shard_map/ppermute | solution.py:637
  24.0 2.2 %collective-permute-start.9 = (bf16[192,1024]{1,0:T(8,128)(2,1)S(1)}, bf16[192,1024]{1,0:T(8,128)(2,1)S(1)}, u32[]{:S(2)}, u32[]{:S(2)}) collective-permute-start(bf16[192,1024]{1,0:T(8,128)(2,1)S(1)} %get-tuple-element.56), channel_id=1, source_target_pairs={{0,1},{1,0},{2,3},{3,2},{4,5},{5,4},{6,7},{7,6},{8,9},{9,8},{10,11... | collective-permute-start | bytes 1179656 | tf_op jit(solution)/shard_map/ppermute | solution.py:627

commit v2 on v1

--- a/solution.py
+++ b/solution.py
@@ -162,11 +162,11 @@
     states = []
     for g in range(vw // 256):
         m = lax.dot_general(
+            decayed[:, g * 128 : (g + 1) * 128],
             v[:, g * 256 : (g + 1) * 256],
-            decayed[:, g * 128 : (g + 1) * 128],
             TN,
             preferred_element_type=F32,
-        )
+        ).T
         states.append(fold(m, dv))
     pack(send, jnp.concatenate(states, axis=1), jnp.exp(running))
 
@@ -329,9 +329,10 @@
             q = query[s, kl].astype(F32) * shrink
             k = key[s, kl].astype(F32)
             end = c[BLOCK - 1 :]
-            q_in = (q * jnp.exp(c)).astype(BF16)
+            grown = q * jnp.exp(c)
+            q_in = grown.astype(BF16)
             k_in = (k * jnp.exp(-c)).astype(BF16)
-            through[s, kl] = (q * jnp.exp(c + base[b : b + 1, kl])).astype(BF16)
+            through[s, kl] = (grown * jnp.exp(base[b : b + 1, kl])).astype(BF16)
             v = val[s, vl]
             k_wide = jnp.where(k_mask, jnp.concatenate([k_in] * 4, axis=0), zero)
             scores = lax.dot_general(q_in, k_wide, NT, preferred_element_type=F32)

time: 27.2 us -> 27.2 us (level)
  no operation moved by 1% of the time
where the time goes in v2:
time: 27.2 us; the launch traced here: 27.1 us
  Pallas kernels  15.4 us (57%)
  starting transfers between devices  9.98 us (37%)
  waiting for transfers between devices  1.19 us (4%)
  local copies, waits for them, and re-layouts  0.34 us (1%)
    pallas_call x10, Pallas kernels, call(): pl.pallas_call(body, out_shape=[jax.ShapeDtypeStruct(s, d) for s, d in ou...  14.4 us
    ppermute x6, starting transfers between devices, on_device(): items[j] = lax.ppermute(payload, ('sp', 'tp'), pairs)  8.07 us
    pallas_call x1, Pallas kernels, on_device(): pl.pallas_call(add_rows, out_shape=jax.ShapeDtypeStruct((rows // 2, model...  0.95 us
    ppermute x6, waiting for transfers between devices, on_device(): items[j] = lax.ppermute(payload, ('sp', 'tp'), pairs)  0.67 us
  transfers between devices with their start and end apart: 11, of which 2 were waited for; matrix products, arithmetic and copies ran while one was open for 0% of the time, Pallas kernels for 38%

profile of v2, /device:TPU:0, one launch (start us, length us, event | category | flops | bytes accessed | tf_op | source)
XLA Modules:
  0.0 27.1 jit_solution(3559365913352038580)
XLA Ops:
  0.0 0.5 %collective-permute-start = (bf16[384,1024]{1,0:T(8,128)(2,1)}, bf16[384,1024]{1,0:T(8,128)(2,1)S(1)}, u32[]{:S(2)}, u32[]{:S(2)}) collective-permute-start(bf16[384,1024]{1,0:T(8,128)(2,1)} %tok_hbm.1), channel_id=1, source_target_pairs={{0,1},{1,0},{2,3},{3,2},{4,5},{5,4},{6,7},{7,6},{8,9},{9,8},{10,11... | collective-permute-start | bytes 2359304 | tf_op jit(solution)/shard_map/ppermute | solution.py:484
  0.5 3.3 %shard_map.163 = (f32[384,1024]{1,0:T(8,128)S(1)}, bf16[384,1024]{1,0:T(8,128)(2,1)S(1)}, f32[384,128]{1,0:T(8,128)S(1)}, f32[384,256]{1,0:T(8,128)S(1)}, bf16[1024,1024]{1,0:T(8,128)(2,1)S(1)}) custom-call(bf16[384,1024]{1,0:T(8,128)(2,1)} %tok_hbm.1, f32[1,2048]{1,0:T(1,128)} %bitcast.6, f32[8,384]{1,0:T(8,128)} %bitcast.10, bf16[2048,256]{1,0:T(8,128)(2,1)} %refs_0_.1, ...), custom_call_target="tpu_custom_call" | custom-call | flops 805306368 | bytes 1048576 | tf_op jit(solution)/shard_map/pallas_call | solution.py:32
  3.8 0.0 collective-permute-done.tok
  3.8 0.0 copy-done.8
  3.8 0.0 copy-done.9
  3.8 0.0 copy-start.2
  3.8 0.0 copy-start.3
  3.8 1.9 %shard_map.164 = (bf16[384,2048]{1,0:T(8,128)(2,1)S(1)}, f32[384,128]{1,0:T(8,128)S(1)}, bf16[384,256]{1,0:T(8,128)(2,1)S(1)}, bf16[384,512]{1,0:T(8,128)(2,1)S(...) custom-call(bf16[384,1024]{1,0:T(8,128)(2,1)S(1)} %collective-permute-done.tok, ...), custom_call_target="tpu_custom_call" | custom-call | flops 805306368 | bytes 1048576 | tf_op jit(solution)/shard_map/pallas_call | solution.py:32
  5.7 0.0 copy-done.2
  5.7 0.3 %copy-done.3 = bf16[2048,512]{1,0:T(8,128)(2,1)S(1)} copy-done((bf16[2048,512]{1,0:T(8,128)(2,1)S(1)}, bf16[2048,512]{1,0:T(8,128)(2,1)}, u32[]{:S(2)}) %copy-start.3) | copy-done | bytes 2097176
  6.0 0.7 %shard_map.165 = bf16[72,256]{1,0:T(8,128)(2,1)S(1)} custom-call(bf16[384,2048]{1,0:T(8,128)(2,1)S(1)} %get-tuple-element.38.full, f32[384,128]{1,0:T(8,128)S(1)} %get-tuple-element.39.scale, bf16[2048,512]{1,0:T(8,128)(2,1)S(1)} %copy-done.2, bf16[2048,512]{1,0:T(8,128)(2,1)S(1)} %copy-done.3, bf16[72,256]{1,0:T(8,128)(2,1)S(1)} %get-tuple-element.37.send), custom_call_target="tpu_custom_call" | custom-call | flops 402653184 | bytes 1048576 | tf_op jit(solution)/shard_map/pallas_call | solution.py:32
  6.7 3.6 %collective-permute-start.4 = (bf16[72,256]{1,0:T(8,128)(2,1)S(1)}, bf16[72,256]{1,0:T(8,128)(2,1)S(1)}, u32[]{:S(2)}, u32[]{:S(2)}) collective-permute-start(bf16[72,256]{1,0:T(8,128)(2,1)S(1)} %shard_map.165), channel_id=1, source_target_pairs={{0,7},{1,6},{2,5},{3,4},{4,3},{5,2},{6,1},{7,0},{8,15},{9,14},{10,... | collective-permute-start | bytes 110600 | tf_op jit(solution)/shard_map/ppermute | solution.py:585
  10.3 0.1 collective-permute-start.2
  10.5 0.1 collective-permute-start.3
  10.6 0.5 %collective-permute-start.1 = (bf16[72,256]{1,0:T(8,128)(2,1)S(1)}, bf16[72,256]{1,0:T(8,128)(2,1)S(1)}, u32[]{:S(2)}, u32[]{:S(2)}) collective-permute-start(bf16[72,256]{1,0:T(8,128)(2,1)S(1)} %get-tuple-element.37.send), channel_id=1, source_target_pairs={{0,1},{1,0},{2,3},{3,2},{4,5},{5,4},{6,7},{7,6},{8,9},{9,8},{10,11... | collective-permute-start | bytes 110600 | tf_op jit(solution)/shard_map/ppermute | solution.py:587
  11.1 0.0 copy-done.10
  11.1 0.0 copy-done.11
  11.1 0.0 copy-start.7
  11.1 2.8 %shard_map.167 = (bf16[384,512]{1,0:T(8,128)(2,1)S(1)}, f32[384,512]{1,0:T(8,128)S(1)}) custom-call(bf16[384,2048]{1,0:T(8,128)(2,1)S(1)} %get-tuple-element.38.full, f32[384,128]{1,0:T(8,128)S(1)} %get-tuple-element.39.scale, bf16[2048,512]{1,0:T(8,128)(2,1)S(1)} %copy-done.2, bf16[2048,512]{1,0:T(8,128)(2,1)S(1)} %copy-done.3, ...), custom_call_target="tpu_custom_call" | custom-call | flops 2415919104 | bytes 1048576 | tf_op jit(solution)/shard_map/pallas_call | solution.py:32
  13.9 0.0 collective-permute-done.4.refs_3_
  13.9 0.0 collective-permute-done.2.refs_1_
  13.9 0.0 collective-permute-done.3.refs_2_
  13.9 0.0 collective-permute-done.1.refs_0_
  13.9 0.1 shard_map.166
  14.0 3.8 %collective-permute-start.7 = (bf16[72,256]{1,0:T(8,128)(2,1)S(1)}, bf16[72,256]{1,0:T(8,128)(2,1)S(1)}, u32[]{:S(2)}, u32[]{:S(2)}) collective-permute-start(bf16[72,256]{1,0:T(8,128)(2,1)S(1)} %get-tuple-element.40.refs_0_), channel_id=1, source_target_pairs={{0,25},{1,24},{2,27},{3,26},{4,29},{5,28},{6,31},{7,30},{8,17},{9,... | collective-permute-start | bytes 110600 | tf_op jit(solution)/shard_map/ppermute | solution.py:585
  17.8 0.0 collective-permute-start.6
  17.8 0.4 %collective-permute-start.5 = (bf16[72,256]{1,0:T(8,128)(2,1)S(1)}, bf16[72,256]{1,0:T(8,128)(2,1)S(1)}, u32[]{:S(2)}, u32[]{:S(2)}) collective-permute-start(bf16[72,256]{1,0:T(8,128)(2,1)S(1)} %get-tuple-element.40.refs_0_), channel_id=1, source_target_pairs={{0,9},{1,8},{2,11},{3,10},{4,13},{5,12},{6,15},{7,14},{8,1},{9,0},... | collective-permute-start | bytes 110600 | tf_op jit(solution)/shard_map/ppermute | solution.py:585
  18.2 0.3 %collective-permute-start.8 = (bf16[72,256]{1,0:T(8,128)(2,1)S(1)}, bf16[72,256]{1,0:T(8,128)(2,1)S(1)}, u32[]{:S(2)}, u32[]{:S(2)}) collective-permute-start(bf16[72,256]{1,0:T(8,128)(2,1)S(1)} %get-tuple-element.41), channel_id=1, source_target_pairs={{0,1},{1,0},{2,3},{3,2},{4,5},{5,4},{6,7},{7,6},{8,9},{9,8},{10,11... | collective-permute-start | bytes 110600 | tf_op jit(solution)/shard_map/ppermute | solution.py:589
  18.5 0.0 copy-done.4
  18.5 0.0 copy-done.5
  18.5 0.0 copy-done.7
  18.6 0.0 copy-start
  18.6 0.0 copy-start.1
  18.6 1.5 %shard_map.168 = (bf16[384,256]{1,0:T(8,128)(2,1)S(1)}, bf16[384,512]{1,0:T(8,128)(2,1)S(1)}, bf16[384,512]{1,0:T(8,128)(2,1)S(1)}) custom-call(bf16[384,2048]{1,0:T(8,128)(2,1)S(1)} %get-tuple-element.38.full, f32[384,128]{1,0:T(8,128)S(1)} %get-tuple-element.39.scale, bf16[3,512]{1,0:T(4,128)(2,1)S(1)} %copy-done.7, bf16[2048,512]{1,0:T(8,128)(2,1)S(1)} %copy-done.4, ...), custom_call_target="tpu_custom_call" | custom-call | flops 1207959552 | bytes 1048576 | tf_op jit(solution)/shard_map/pallas_call | solution.py:32
  20.1 1.5 %shard_map.169 = (f32[384,512]{1,0:T(8,128)S(1)}, bf16[384,256]{1,0:T(8,128)(2,1)S(1)}, f32[64,256]{1,0:T(8,128)S(1)}) custom-call(bf16[384,256]{1,0:T(8,128)(2,1)S(1)} %get-tuple-element.43.query, bf16[384,256]{1,0:T(8,128)(2,1)S(1)} %get-tuple-element.44.key, bf16[384,512]{1,0:T(8,128)(2,1)S(1)} %get-tuple-element.45.val, ...), custom_call_target="tpu_custom_call" | custom-call | flops 16777216 | bytes 1048576 | tf_op jit(solution)/shard_map/pallas_call | solution.py:32
  21.6 0.0 collective-permute-done.8.refs_4_
  21.6 0.0 collective-permute-done.7.refs_3_
  21.6 0.6 %collective-permute-done.6.refs_2_ = bf16[72,256]{1,0:T(8,128)(2,1)S(1)} collective-permute-done((bf16[72,256]{1,0:T(8,128)(2,1)S(1)}, bf16[72,256]{1,0:T(8,128)(2,1)S(1)}, u32[]{:S(2)}, u32[]{:S(2)}) %collective-permute-start.6) | collective-permute-done | bytes 36896 | tf_op jit(solution)/shard_map/ppermute | solution.py:585
  22.3 0.0 collective-permute-done.5.refs_1_
  22.3 0.0 copy-done.1
  22.3 0.9 %shard_map.170 = (bf16[192,1024]{1,0:T(8,128)(2,1)S(1)}, bf16[192,512]{1,0:T(8,128)(2,1)S(1)}, bf16[192,512]{1,0:T(8,128)(2,1)S(1)}, bf16[2,256,128]{2,1,0:T(8,128)(2,1)S(1)}, f32[8,512]{1,0:T(8,128)S(1)}) custom-call(bf16[72,256]{1,0:T(8,128)(2,1)S(1)} %get-tuple-element.40.refs_0_, bf16[72,256]{1,0:T(8,128)(2,1)S(1)} %collective-permute-done.5.refs_1_, ...), custom_call_target="tpu_custom_call" | custom-call | flops 402653184 | bytes 1048576 | tf_op jit(solution)/shard_map/pallas_call | solution.py:32
  23.2 0.6 %shard_map.172 = bf16[192,1024]{1,0:T(8,128)(2,1)S(1)} custom-call(bf16[192,512]{1,0:T(8,128)(2,1)S(1)} %get-tuple-element.57.left, bf16[192,512]{1,0:T(8,128)(2,1)S(1)} %get-tuple-element.58.attn, bf16[512,2048]{1,0:T(8,128)(2,1)S(1)} %copy-done, bf16[512,2048]{1,0:T(8,128)(2,1)S(1)} %copy-done.1), custom_call_target="tpu_custom_call" | custom-call | flops 402653184 | bytes 1048576 | tf_op jit(solution)/shard_map/pallas_call | solution.py:32
  23.8 0.2 collective-permute-start.10
  24.0 0.4 %collective-permute-start.9 = (bf16[192,1024]{1,0:T(8,128)(2,1)S(1)}, bf16[192,1024]{1,0:T(8,128)(2,1)S(1)}, u32[]{:S(2)}, u32[]{:S(2)}) collective-permute-start(bf16[192,1024]{1,0:T(8,128)(2,1)S(1)} %get-tuple-element.56), channel_id=1, source_target_pairs={{0,1},{1,0},{2,3},{3,2},{4,5},{5,4},{6,7},{7,6},{8,9},{9,8},{10,11... | collective-permute-start | bytes 1179656 | tf_op jit(solution)/shard_map/ppermute | solution.py:628
  24.4 1.2 %shard_map.171.mine = f32[192,2048]{1,0:T(8,128)S(1)} custom-call(bf16[2,256,128]{2,1,0:T(8,128)(2,1)S(1)} %get-tuple-element.54.state, f32[8,512]{1,0:T(8,128)S(1)} %get-tuple-element.55.halo, f32[384,512]{1,0:T(8,128)S(1)} %get-tuple-element.49.refs_6_.raw, bf16[384,256]{1,0:T(8,128)(2,1)S(1)} %get-tuple-element.50.refs_7_.through, ...), custom_call_target="tpu_custom_call" | custom-call | flops 805306368 | bytes 1048576 | tf_op jit(solution)/shard_map/pallas_call | solution.py:32
  25.6 0.0 collective-permute-done.10.second
  25.6 0.5 %collective-permute-done.9.first = bf16[192,1024]{1,0:T(8,128)(2,1)S(1)} collective-permute-done((bf16[192,1024]{1,0:T(8,128)(2,1)S(1)}, bf16[192,1024]{1,0:T(8,128)(2,1)S(1)}, u32[]{:S(2)}, u32[]{:S(2)}) %collective-permute-start.9) | collective-permute-done | bytes 393248 | tf_op jit(solution)/shard_map/ppermute | solution.py:628
  26.1 0.9 %add_rows.1 = bf16[192,2048]{1,0:T(8,128)(2,1)} custom-call(f32[192,2048]{1,0:T(8,128)S(1)} %shard_map.171.mine, bf16[192,1024]{1,0:T(8,128)(2,1)S(1)} %collective-permute-done.9.first, bf16[192,1024]{1,0:T(8,128)(2,1)S(1)} %collective-permute-done.10.second), custom_call_target="tpu_custom_call" | custom-call | flops 1048576 | bytes 1048576 | tf_op jit(solution)/shard_map/add_rows/pallas_call | solution.py:642
  (9 shorter events, 0.0 us)
Async XLA Ops:
  0.0 3.8 %collective-permute-start = (bf16[384,1024]{1,0:T(8,128)(2,1)}, bf16[384,1024]{1,0:T(8,128)(2,1)S(1)}, u32[]{:S(2)}, u32[]{:S(2)}) collective-permute-start(bf16[384,1024]{1,0:T(8,128)(2,1)} %tok_hbm.1), channel_id=1, source_target_pairs={{0,1},{1,0},{2,3},{3,2},{4,5},{5,4},{6,7},{7,6},{8,9},{9,8},{10,11... | collective-permute-start | bytes 2359304 | tf_op jit(solution)/shard_map/ppermute | solution.py:484
  0.5 3.3 %copy-start.8 = (f32[2048]{0:T(1024)S(1)}, f32[2048]{0:T(1024)}, u32[]{:S(2)}) copy-start(f32[2048]{0:T(1024)} %param.18) | copy-start | bytes 24580
  0.5 3.3 %copy-start.9 = (f32[256]{0:T(256)S(1)}, f32[256]{0:T(256)}, u32[]{:S(2)}) copy-start(f32[256]{0:T(256)} %param.28) | copy-start | bytes 3076
  3.8 1.9 %copy-start.2 = (bf16[2048,512]{1,0:T(8,128)(2,1)S(1)}, bf16[2048,512]{1,0:T(8,128)(2,1)}, u32[]{:S(2)}) copy-start(bf16[2048,512]{1,0:T(8,128)(2,1)} %wc.5) | copy-start | bytes 6291460
  3.8 2.2 %copy-start.3 = (bf16[2048,512]{1,0:T(8,128)(2,1)S(1)}, bf16[2048,512]{1,0:T(8,128)(2,1)}, u32[]{:S(2)}) copy-start(bf16[2048,512]{1,0:T(8,128)(2,1)} %wh.3) | copy-start | bytes 6291460
  6.0 5.1 %copy-start.10 = (bf16[2048,512]{1,0:T(8,128)(2,1)S(1)}, bf16[2048,512]{1,0:T(8,128)(2,1)}, u32[]{:S(2)}) copy-start(bf16[2048,512]{1,0:T(8,128)(2,1)} %wg.1) | copy-start | bytes 6291460
  6.0 5.1 %copy-start.11 = (f32[64]{0:T(128)S(1)}, f32[64]{0:T(128)}, u32[]{:S(2)}) copy-start(f32[64]{0:T(128)} %param.31) | copy-start | bytes 772
  6.7 7.2 %collective-permute-start.4 = (bf16[72,256]{1,0:T(8,128)(2,1)S(1)}, bf16[72,256]{1,0:T(8,128)(2,1)S(1)}, u32[]{:S(2)}, u32[]{:S(2)}) collective-permute-start(bf16[72,256]{1,0:T(8,128)(2,1)S(1)} %shard_map.165), channel_id=1, source_target_pairs={{0,7},{1,6},{2,5},{3,4},{4,3},{5,2},{6,1},{7,0},{8,15},{9,14},{10,... | collective-permute-start | bytes 110600 | tf_op jit(solution)/shard_map/ppermute | solution.py:585
  10.3 3.6 %collective-permute-start.2 = (bf16[72,256]{1,0:T(8,128)(2,1)S(1)}, bf16[72,256]{1,0:T(8,128)(2,1)S(1)}, u32[]{:S(2)}, u32[]{:S(2)}) collective-permute-start(bf16[72,256]{1,0:T(8,128)(2,1)S(1)} %shard_map.165), channel_id=1, source_target_pairs={{0,3},{1,2},{2,1},{3,0},{4,7},{5,6},{6,5},{7,4},{8,11},{9,10},{10,... | collective-permute-start | bytes 110600 | tf_op jit(solution)/shard_map/ppermute | solution.py:585
  10.5 3.5 %collective-permute-start.3 = (bf16[72,256]{1,0:T(8,128)(2,1)S(1)}, bf16[72,256]{1,0:T(8,128)(2,1)S(1)}, u32[]{:S(2)}, u32[]{:S(2)}) collective-permute-start(bf16[72,256]{1,0:T(8,128)(2,1)S(1)} %get-tuple-element.37.send), channel_id=1, source_target_pairs={{0,5},{1,4},{2,7},{3,6},{4,1},{5,0},{6,3},{7,2},{8,13},{9,12},{10,... | collective-permute-start | bytes 110600 | tf_op jit(solution)/shard_map/ppermute | solution.py:585
  10.6 3.3 %collective-permute-start.1 = (bf16[72,256]{1,0:T(8,128)(2,1)S(1)}, bf16[72,256]{1,0:T(8,128)(2,1)S(1)}, u32[]{:S(2)}, u32[]{:S(2)}) collective-permute-start(bf16[72,256]{1,0:T(8,128)(2,1)S(1)} %get-tuple-element.37.send), channel_id=1, source_target_pairs={{0,1},{1,0},{2,3},{3,2},{4,5},{5,4},{6,7},{7,6},{8,9},{9,8},{10,11... | collective-permute-start | bytes 110600 | tf_op jit(solution)/shard_map/ppermute | solution.py:587
  11.1 7.5 %copy-start.4 = (bf16[2048,512]{1,0:T(8,128)(2,1)S(1)}, bf16[2048,512]{1,0:T(8,128)(2,1)}, u32[]{:S(2)}) copy-start(bf16[2048,512]{1,0:T(8,128)(2,1)} %wb.1) | copy-start | bytes 6291460
  11.1 7.5 %copy-start.5 = (bf16[2048,256]{1,0:T(8,128)(2,1)S(1)}, bf16[2048,256]{1,0:T(8,128)(2,1)}, u32[]{:S(2)}) copy-start(bf16[2048,256]{1,0:T(8,128)(2,1)} %wq.1) | copy-start | bytes 3145732
  11.1 7.5 %copy-start.7 = (bf16[3,512]{1,0:T(4,128)(2,1)S(1)}, bf16[3,512]{1,0:T(4,128)(2,1)}, u32[]{:S(2)}) copy-start(bf16[3,512]{1,0:T(4,128)(2,1)} %taps.3) | copy-start | bytes 9220
  14.0 7.6 %collective-permute-start.7 = (bf16[72,256]{1,0:T(8,128)(2,1)S(1)}, bf16[72,256]{1,0:T(8,128)(2,1)S(1)}, u32[]{:S(2)}, u32[]{:S(2)}) collective-permute-start(bf16[72,256]{1,0:T(8,128)(2,1)S(1)} %get-tuple-element.40.refs_0_), channel_id=1, source_target_pairs={{0,25},{1,24},{2,27},{3,26},{4,29},{5,28},{6,31},{7,30},{8,17},{9,... | collective-permute-start | bytes 110600 | tf_op jit(solution)/shard_map/ppermute | solution.py:585
  17.8 4.5 %collective-permute-start.6 = (bf16[72,256]{1,0:T(8,128)(2,1)S(1)}, bf16[72,256]{1,0:T(8,128)(2,1)S(1)}, u32[]{:S(2)}, u32[]{:S(2)}) collective-permute-start(bf16[72,256]{1,0:T(8,128)(2,1)S(1)} %get-tuple-element.40.refs_0_), channel_id=1, source_target_pairs={{0,17},{1,16},{2,19},{3,18},{4,21},{5,20},{6,23},{7,22},{8,25},{9,... | collective-permute-start | bytes 110600 | tf_op jit(solution)/shard_map/ppermute | solution.py:585
  17.8 4.5 %collective-permute-start.5 = (bf16[72,256]{1,0:T(8,128)(2,1)S(1)}, bf16[72,256]{1,0:T(8,128)(2,1)S(1)}, u32[]{:S(2)}, u32[]{:S(2)}) collective-permute-start(bf16[72,256]{1,0:T(8,128)(2,1)S(1)} %get-tuple-element.40.refs_0_), channel_id=1, source_target_pairs={{0,9},{1,8},{2,11},{3,10},{4,13},{5,12},{6,15},{7,14},{8,1},{9,0},... | collective-permute-start | bytes 110600 | tf_op jit(solution)/shard_map/ppermute | solution.py:585
  18.2 3.4 %collective-permute-start.8 = (bf16[72,256]{1,0:T(8,128)(2,1)S(1)}, bf16[72,256]{1,0:T(8,128)(2,1)S(1)}, u32[]{:S(2)}, u32[]{:S(2)}) collective-permute-start(bf16[72,256]{1,0:T(8,128)(2,1)S(1)} %get-tuple-element.41), channel_id=1, source_target_pairs={{0,1},{1,0},{2,3},{3,2},{4,5},{5,4},{6,7},{7,6},{8,9},{9,8},{10,11... | collective-permute-start | bytes 110600 | tf_op jit(solution)/shard_map/ppermute | solution.py:589
  18.5 1.5 %copy-start.6 = (f32[8,32,64]{2,1,0:T(8,128)S(1)}, f32[8,32,64]{2,1,0:T(8,128)}, u32[]{:S(2)}) copy-start(f32[8,32,64]{2,1,0:T(8,128)} %param.30) | copy-start | bytes 196612
  18.6 3.7 %copy-start = (bf16[512,2048]{1,0:T(8,128)(2,1)S(1)}, bf16[512,2048]{1,0:T(8,128)(2,1)}, u32[]{:S(2)}) copy-start(bf16[512,2048]{1,0:T(8,128)(2,1)} %wc.7) | copy-start | bytes 6291460
  18.6 3.7 %copy-start.1 = (bf16[512,2048]{1,0:T(8,128)(2,1)S(1)}, bf16[512,2048]{1,0:T(8,128)(2,1)}, u32[]{:S(2)}) copy-start(bf16[512,2048]{1,0:T(8,128)(2,1)} %wa.3) | copy-start | bytes 6291460
  23.8 1.8 %collective-permute-start.10 = (bf16[192,1024]{1,0:T(8,128)(2,1)S(1)}, bf16[192,1024]{1,0:T(8,128)(2,1)S(1)}, u32[]{:S(2)}, u32[]{:S(2)}) collective-permute-start(bf16[192,1024]{1,0:T(8,128)(2,1)S(1)} %shard_map.172), channel_id=1, source_target_pairs={{0,1},{1,0},{2,3},{3,2},{4,5},{5,4},{6,7},{7,6},{8,9},{9,8},{10,11... | collective-permute-start | bytes 1179656 | tf_op jit(solution)/shard_map/ppermute | solution.py:638
  24.0 2.2 %collective-permute-start.9 = (bf16[192,1024]{1,0:T(8,128)(2,1)S(1)}, bf16[192,1024]{1,0:T(8,128)(2,1)S(1)}, u32[]{:S(2)}, u32[]{:S(2)}) collective-permute-start(bf16[192,1024]{1,0:T(8,128)(2,1)S(1)} %get-tuple-element.56), channel_id=1, source_target_pairs={{0,1},{1,0},{2,3},{3,2},{4,5},{5,4},{6,7},{7,6},{8,9},{9,8},{10,11... | collective-permute-start | bytes 1179656 | tf_op jit(solution)/shard_map/ppermute | solution.py:628
